TPU v7x, 32 devices: a whole 2x2x4 slice. The times are simulated.
32 devices in a mesh: grp: 2 (over y), tp: 4 (over z), dp: 4 (over x, core).
Axes of the slice: x: 2, y: 2, z: 4, core: 2. Of those that a mesh axis runs over, the one named last changes fastest.
Arguments:
- tokens: bfloat16 [64, 8, 4096], P(('grp', 'tp'), None, 'dp'), parts along dimension 0, may hold values from -6 to 6
- lengths: int32 [64], P('grp'), parts along dimension 0, may hold values from 1 to 8, 112 in all
- norm_gain: float32 [2, 4096], P(None, 'dp'), may hold values from 0.1 to 1.9
- w_recept: bfloat16 [2, 4096, 2048], P(None, 'dp', 'tp'), may hold values from -0.09375 to 0.09375
- w_key: bfloat16 [2, 4096, 2048], P(None, 'dp', 'tp'), may hold values from -0.09375 to 0.09375
- w_value: bfloat16 [2, 4096, 2048], P(None, 'dp', 'tp'), may hold values from -0.09375 to 0.09375
- w_decay: bfloat16 [2, 4096, 2048], P(None, 'dp', 'tp'), may hold values from -0.375 to 0.375
- w_rate: bfloat16 [2, 4096, 2048], P(None, 'dp', 'tp'), may hold values from -0.09375 to 0.09375
- w_gate: bfloat16 [2, 4096, 2048], P(None, 'dp', 'tp'), may hold values from -0.09375 to 0.09375
- w_out: bfloat16 [2, 2048, 4096], P(None, 'tp', 'dp'), may hold values from -0.125 to 0.125
- decay_base: float32 [2, 2048], P(None, 'tp'), may hold values from -4 to 3
- out_gain: float32 [2, 2048], P(None, 'tp'), may hold values from 0.1 to 1.9
- states: float32 [2, 64, 64, 2048], P(None, ('grp', 'dp'), None, 'tp'), parts along dimension 1, may hold values from -6 to 6
Outputs:
- stream_out: float32 [64, 8, 4096], P(('grp', 'tp'), None, 'dp'), parts along dimension 0
- new_states: float32 [2, 64, 64, 2048], P(None, ('grp', 'dp'), None, 'tp'), parts along dimension 1
There are 2 independent parts, one for each index of `grp`. A program takes and returns all parts, laid end to end along the dimension named above; an argument that names none is the same for every part. Nothing has to cross between parts.
Inputs may be any that keep to these rules, and one draw needn't show every extreme that they name: lengths[b] first tokens of sequence b are live; together they count 7 * 16 and the largest is 8.
All inputs are finite; a program needn't handle non-finite values.
Results may differ from a plain program's by a relative error of at most 0.0061.
Values may be sent and summed in bfloat16 or wider, within the bound.
A program may use at most 128 MiB of HBM per device.

v0:
```python
import functools

import jax
import jax.numpy as jnp
from jax import lax
from jax.experimental import pallas as pl
from jax.experimental.pallas import tpu as pltpu
from jax.sharding import PartitionSpec as P

HEAD = 64
BLOCKS = 2
LANES = 128
CORES = 2

group_eps = 0.00064
norm_eps = 1e-06
key_eps = 1e-06
decay_scale = 0.606531
MESH = pl.DeviceIdType.MESH
F32 = jnp.float32
BF16 = jnp.bfloat16


def remote(src, dst, send, recv, axis, peer):
    return pltpu.make_async_remote_copy(
        src_ref=src,
        dst_ref=dst,
        send_sem=send,
        recv_sem=recv,
        device_id={axis: peer},
        device_id_type=MESH,
    )


def greet(peers):
    barrier = pltpu.get_barrier_semaphore()
    for axis, peer in peers:
        pl.semaphore_signal(barrier, inc=1, device_id={axis: peer}, device_id_type=MESH)
    pl.semaphore_wait(barrier, len(peers))


def project_kernel(
    block, ntp, ndp, rows, width,
    x_ref, gain_ref, w0, w1, w2, w3, w4, w5,
    out_ref, total_ref,
    wbuf, xg, sqg, part, send_a, recv_a, send_b, recv_b, sq_a, sq_ra, sq_b, sq_rb,
    wsem, xs_sem, xr_sem, ss_sem, sr_sem, as_sem, ar_sem, bs_sem, br_sem,
    qas_sem, qar_sem, qbs_sem, qbr_sem,
):
    weights = (w0, w1, w2, w3, w4, w5)
    chunks, depth, _ = wbuf.shape
    halves = chunks // 6
    nx = ndp // CORES
    tp = lax.axis_index("tp")
    dp = lax.axis_index("dp")
    core = lax.rem(dp, CORES)
    xpos = dp // CORES
    partner = dp + 1 - 2 * core

    def load(c):
        return pltpu.make_async_copy(
            weights[c // halves].at[block, :, pl.ds((c % halves) * width, width)],
            wbuf.at[c],
            wsem.at[c],
        )

    for c in range(chunks):
        load(c).start()
    x = x_ref[...].astype(F32)
    xg[tp] = (x * gain_ref[...]).astype(BF16)
    sq = x * x
    acc = sq[:, 0:LANES]
    for k in range(1, depth // LANES):
        acc = acc + sq[:, k * LANES : (k + 1) * LANES]
    sqg[tp] = acc
    peers = [("tp", lax.rem(tp + k, ntp)) for k in range(1, ntp)]
    peers += [("dp", partner)]
    peers += [("dp", CORES * lax.rem(xpos + k, nx) + core) for k in range(1, nx)]
    greet(peers)

    gathers = []
    for k in range(1, ntp):
        peer = lax.rem(tp + k, ntp)
        cp = remote(xg.at[tp], xg.at[tp], xs_sem.at[k], xr_sem.at[k], "tp", peer)
        cq = remote(sqg.at[tp], sqg.at[tp], ss_sem.at[k], sr_sem.at[k], "tp", peer)
        cp.start()
        cq.start()
        gathers += [cp, cq]
    for k in range(1, ntp):
        src = lax.rem(tp + ntp - k, ntp)
        remote(xg.at[src], xg.at[src], xs_sem.at[k], xr_sem.at[k], "tp", src).wait_recv()
        remote(sqg.at[src], sqg.at[src], ss_sem.at[k], sr_sem.at[k], "tp", src).wait_recv()

    sq_all = sqg[...].reshape(ndp, rows, LANES)
    part_sq = [sq_all[d] for d in range(ndp)]

    def pick(parts, x_at, which):
        return jnp.where(which == 0, parts[CORES * x_at], parts[CORES * x_at + 1])

    for xd in range(nx):
        sq_a[xd] = pick(part_sq, xd, 1 - core)
        sq_b[xd] = pick(part_sq, xd, core)
    copy_qa = remote(sq_a, sq_ra, qas_sem, qar_sem, "dp", partner)
    copy_qa.start()

    def copy_a(c):
        return remote(send_a.at[c], recv_a.at[c], as_sem.at[c], ar_sem.at[c], "dp", partner)

    def copy_b(c, k):
        xd = lax.rem(xpos + k, nx)
        return remote(
            send_b.at[c, k], recv_b.at[c, k], bs_sem.at[c, k], br_sem.at[c, k],
            "dp", CORES * xd + core,
        )

    def stage_b(c):
        copy_a(c).wait_recv()
        for k in range(1, nx):
            xd = lax.rem(xpos + k, nx)
            send_b[c, k] = (part[c, CORES * xd + core] + recv_a[c, xd].astype(F32)).astype(BF16)
            copy_b(c, k).start()

    def first(c, carry):
        pltpu.make_async_copy(wbuf.at[c], wbuf.at[c], wsem.at[c]).wait()
        res = jnp.dot(
            xg[...].reshape(ndp * rows, depth), wbuf[c], preferred_element_type=F32
        )
        part[c] = res.reshape(ndp, rows, width)
        for xd in range(nx):
            send_a[c, xd] = part[c, CORES * xd + 1 - core].astype(BF16)
        copy_a(c).start()

        @pl.when(c > 0)
        def _():
            stage_b(c - 1)

        return carry

    lax.fori_loop(0, chunks, first, 0)
    copy_qa.wait_recv()
    for xd in range(nx):
        sq_b[xd] = sq_b[xd] + sq_ra[xd]
    qb = []
    for k in range(1, nx):
        xd = lax.rem(xpos + k, nx)
        cp = remote(
            sq_b.at[xd], sq_rb.at[k], qbs_sem.at[k], qbr_sem.at[k], "dp", CORES * xd + core
        )
        cp.start()
        qb.append(cp)
    stage_b(chunks - 1)

    def last(c, carry):
        own = part[c, CORES * xpos + core] + recv_a[c, xpos].astype(F32)
        for k in range(1, nx):
            copy_b(c, k).wait_recv()
            own = own + recv_b[c, k].astype(F32)
        out_ref[:, pl.ds(pl.multiple_of(c * width, width), width)] = own
        copy_a(c).wait_send()
        for k in range(1, nx):
            copy_b(c, k).wait_send()
        return carry

    lax.fori_loop(0, chunks, last, 0)
    total = sq_b[xpos]
    for k in range(1, nx):
        qb[k - 1].wait_recv()
        total = total + sq_rb[k]
    total_ref[...] = total
    copy_qa.wait_send()
    for cp in qb:
        cp.wait_send()
    for cp in gathers:
        cp.wait_send()


def project(block, ntp, ndp, rows, x, gain, weights, ident):
    here, depth = x.shape
    span = weights[0].shape[2]
    width = min(256, span)
    chunks = 6 * span // width
    nx = ndp // CORES
    dma = pltpu.SemaphoreType.DMA
    vmem = pl.BlockSpec(memory_space=pltpu.VMEM)
    hbm = pl.BlockSpec(memory_space=pl.ANY)
    return pl.pallas_call(
        functools.partial(project_kernel, block, ntp, ndp, rows, width),
        out_shape=(
            jax.ShapeDtypeStruct((rows, 6 * span), F32),
            jax.ShapeDtypeStruct((rows, LANES), F32),
        ),
        in_specs=[vmem, vmem] + [hbm] * 6,
        out_specs=(vmem, vmem),
        scratch_shapes=[
            pltpu.VMEM((chunks, depth, width), BF16),
            pltpu.VMEM((ntp, here, depth), BF16),
            pltpu.VMEM((ntp, here, LANES), F32),
            pltpu.VMEM((chunks, ndp, rows, width), F32),
            pltpu.VMEM((chunks, nx, rows, width), BF16),
            pltpu.VMEM((chunks, nx, rows, width), BF16),
            pltpu.VMEM((chunks, nx, rows, width), BF16),
            pltpu.VMEM((chunks, nx, rows, width), BF16),
            pltpu.VMEM((nx, rows, LANES), F32),
            pltpu.VMEM((nx, rows, LANES), F32),
            pltpu.VMEM((nx, rows, LANES), F32),
            pltpu.VMEM((nx, rows, LANES), F32),
            dma((chunks,)),
            dma((ntp,)), dma((ntp,)), dma((ntp,)), dma((ntp,)),
            dma((chunks,)), dma((chunks,)),
            dma((chunks, nx)), dma((chunks, nx)),
            dma, dma, dma((nx,)), dma((nx,)),
        ],
        compiler_params=pltpu.CompilerParams(
            collective_id=ident, has_side_effects=True, vmem_limit_bytes=48 * 1024 * 1024
        ),
        name="project%d" % block,
    )(x, gain, *weights)


def split_dot(a, b):
    hi = a.astype(BF16)
    lo = (a - hi.astype(F32)).astype(BF16)
    return jnp.dot(hi, b, preferred_element_type=F32) + jnp.dot(lo, b, preferred_element_type=F32)


def split_dot_right(a, b):
    hi = b.astype(BF16)
    lo = (b - hi.astype(F32)).astype(BF16)
    return jnp.dot(a, hi, preferred_element_type=F32) + jnp.dot(a, lo, preferred_element_type=F32)


def grid_of(shape, dim):
    return lax.broadcasted_iota(jnp.int32, shape, dim)


def mix_kernel(features, steps, proj_ref, total_ref, live_ref, base_ref, gain_ref, state_ref, *rest):
    gated_ref, final_ref = rest[-2], rest[-1]
    rows = proj_ref.shape[0]
    span = base_ref.shape[1]
    heads = span // HEAD
    tall = heads * steps
    inv = lax.rsqrt(jnp.sum(total_ref[...], axis=1, keepdims=True) / features + norm_eps)
    recept, keys, values, decay_pre, rate_pre, gate_pre = (
        proj_ref[:, i * span : (i + 1) * span] * inv for i in range(6)
    )
    live = live_ref[...][:, 0:1]
    seg = (grid_of((span, span), 0) // HEAD == grid_of((span, span), 1) // HEAD).astype(F32).astype(BF16)
    rb = grid_of((rows, rows), 0)
    cb = grid_of((rows, rows), 1)
    same = rb // steps == cb // steps
    lower = jnp.where(same & (cb <= rb), 1.0, 0.0).astype(BF16)
    whole = jnp.where(same, 1.0, 0.0).astype(BF16)
    unit = keys * lax.rsqrt(split_dot(keys * keys, seg) + key_eps)
    removal = unit * jax.nn.sigmoid(rate_pre) * live
    logd = -decay_scale * jax.nn.sigmoid(decay_pre + base_ref[...]) * live
    upto = split_dot_right(lower, logd)
    ends = jnp.exp(split_dot_right(whole, logd))
    back = jnp.exp(-upto)
    u_in = unit * jnp.exp(upto - logd)
    q_in = recept * jnp.exp(upto)
    r_out = removal * back
    k_out = keys * live * back
    r_end = r_out * ends
    k_end = k_out * ends
    scale_out = gain_ref[...] * jax.nn.sigmoid(gate_pre) * live

    mask = jnp.where(
        grid_of((tall, span), 0) // steps == grid_of((tall, span), 1) // HEAD, 1.0, 0.0
    )
    fold = jnp.where(
        grid_of((span, HEAD), 0) % HEAD == grid_of((span, HEAD), 1), 1.0, 0.0
    ).astype(BF16)
    tr = grid_of((tall, tall), 0)
    tc = grid_of((tall, tall), 1)
    strict_m = jnp.where(tc < tr, 1.0, 0.0)
    lower_m = jnp.where(tc <= tr, 1.0, 0.0)
    nt = (((1,), (1,)), ((), ()))
    tn = (((0,), (0,)), ((), ()))

    def exact(a, b):
        return jnp.dot(a, b, preferred_element_type=F32, precision=lax.Precision.HIGHEST)

    def quick(a, b, dims=(((1,), (0,)), ((), ()))):
        return lax.dot_general(a.astype(BF16), b.astype(BF16), dims, preferred_element_type=F32)

    for b in range(rows // steps):
        cut = slice(b * steps, (b + 1) * steps)

        def spread(a):
            return (jnp.concatenate([a[cut]] * heads, axis=0) * mask).astype(BF16)

        memory = state_ref[0, b]
        ask = jnp.concatenate([spread(u_in), spread(q_in)], axis=0)
        on_s = quick(ask, memory, nt)
        on_r = quick(ask, spread(r_out), nt)
        on_k = quick(ask, spread(k_out), nt)
        m1 = on_r[:tall] * strict_m
        m2 = on_k[:tall] * strict_m
        p_r = on_r[tall:] * lower_m
        p_k = on_k[tall:] * lower_m
        vals = jnp.dot(spread(values), fold, preferred_element_type=F32)
        seen = on_s[:tall] + quick(m2, vals)
        squared = exact(m1, m1)
        fourth = exact(squared, squared)
        seen = seen + exact(fourth, seen)
        seen = seen + exact(squared, seen)
        seen = seen - exact(m1, seen)
        read = on_s[tall:] + quick(p_k, vals) - quick(p_r, seen)
        final_ref[0, b] = (
            memory * ends[b * steps : b * steps + 1]
            + quick(vals, spread(k_end), tn)
            - quick(seen, spread(r_end), tn)
        )
        centered = read - jnp.mean(read, axis=1, keepdims=True)
        normed = centered * lax.rsqrt(
            jnp.mean(centered * centered, axis=1, keepdims=True) + group_eps
        )
        wide = jnp.concatenate([normed, normed], axis=1)
        wide = jnp.concatenate([wide] * (heads // 2), axis=1) * mask
        flat = wide[0:steps]
        for h in range(1, heads):
            flat = flat + wide[h * steps : (h + 1) * steps]
        gated_ref[cut, :] = (flat * scale_out[cut]).astype(BF16)


def mix(block, features, steps, proj, total, live, base, gain, states, earlier):
    rows = proj.shape[0]
    span = base.shape[1]
    _, held, size, _ = states.shape
    full = lambda shape: pl.BlockSpec(shape, lambda i: (0,) * len(shape))
    slab = pl.BlockSpec((1, held, size, span), lambda i: (block, 0, 0, 0))
    args = [proj, total, live, base, gain, states]
    in_specs = [full(a.shape) for a in args[:5]] + [slab]
    aliases = {}
    if earlier is not None:
        args.append(earlier)
        in_specs.append(pl.BlockSpec(memory_space=pl.ANY))
        aliases = {6: 1}
    return pl.pallas_call(
        functools.partial(mix_kernel, features, steps),
        grid=(1,),
        out_shape=(
            jax.ShapeDtypeStruct((rows, span), BF16),
            jax.ShapeDtypeStruct(states.shape, F32),
        ),
        in_specs=in_specs,
        out_specs=(full((rows, span)), slab),
        input_output_aliases=aliases,
        compiler_params=pltpu.CompilerParams(vmem_limit_bytes=48 * 1024 * 1024),
        name="mix%d" % block,
    )(*args)


def output_kernel(
    block, ntp, ndp, rows,
    gated_ref, x_ref, w_ref, out_ref,
    wbuf, gg, osend, orecv, wsem, gs_sem, gr_sem, os_sem, or_sem,
):
    here = x_ref.shape[0]
    tp = lax.axis_index("tp")
    dp = lax.axis_index("dp")
    load = pltpu.make_async_copy(w_ref.at[block], wbuf, wsem)
    load.start()
    gg[pl.ds(pl.multiple_of(dp * rows, rows), rows), :] = gated_ref[...]
    greet(
        [("dp", lax.rem(dp + k, ndp)) for k in range(1, ndp)]
        + [("tp", lax.rem(tp + k, ntp)) for k in range(1, ntp)]
    )
    sends = []
    for k in range(1, ndp):
        at = gg.at[pl.ds(pl.multiple_of(dp * rows, rows), rows), :]
        cp = remote(gated_ref, at, gs_sem.at[k], gr_sem.at[k], "dp", lax.rem(dp + k, ndp))
        cp.start()
        sends.append(cp)
    for k in range(1, ndp):
        src = lax.rem(dp + ndp - k, ndp)
        at = gg.at[pl.ds(pl.multiple_of(src * rows, rows), rows), :]
        remote(gated_ref, at, gs_sem.at[k], gr_sem.at[k], "dp", src).wait_recv()
    load.wait()

    def partial_of(peer):
        take = gg[pl.ds(pl.multiple_of(peer * here, here), here), :]
        return jnp.dot(take, wbuf[...], preferred_element_type=F32)

    def copy_o(k):
        return remote(
            osend.at[k], orecv.at[k], os_sem.at[k], or_sem.at[k], "tp", lax.rem(tp + k, ntp)
        )

    def give(k, carry):
        osend[k] = partial_of(lax.rem(tp + k, ntp)).astype(BF16)
        copy_o(k).start()
        return carry

    lax.fori_loop(1, ntp, give, 0)
    out_ref[...] = x_ref[...].astype(F32) + partial_of(tp)

    def take(k, carry):
        copy_o(k).wait_recv()
        out_ref[...] += orecv[k].astype(F32)
        copy_o(k).wait_send()
        return carry

    lax.fori_loop(1, ntp, take, 0)
    for cp in sends:
        cp.wait_send()


def output(block, ntp, ndp, gated, x, w_out, ident):
    rows, span = gated.shape
    here, depth = x.shape
    dma = pltpu.SemaphoreType.DMA
    vmem = pl.BlockSpec(memory_space=pltpu.VMEM)
    return pl.pallas_call(
        functools.partial(output_kernel, block, ntp, ndp, rows),
        out_shape=jax.ShapeDtypeStruct((here, depth), F32),
        in_specs=[vmem, vmem, pl.BlockSpec(memory_space=pl.ANY)],
        out_specs=vmem,
        scratch_shapes=[
            pltpu.VMEM((span, depth), BF16),
            pltpu.VMEM((ndp * rows, span), BF16),
            pltpu.VMEM((ntp, here, depth), BF16),
            pltpu.VMEM((ntp, here, depth), BF16),
            dma,
            dma((ndp,)), dma((ndp,)), dma((ntp,)), dma((ntp,)),
        ],
        compiler_params=pltpu.CompilerParams(
            collective_id=ident, has_side_effects=True, vmem_limit_bytes=48 * 1024 * 1024
        ),
        name="output%d" % block,
    )(gated, x, w_out)


def body(
    ntp, ndp,
    tokens, lengths, norm_gain,
    w_recept, w_key, w_value, w_decay, w_rate, w_gate,
    w_out, decay_base, out_gain, states,
):
    seqs, steps, depth = tokens.shape
    held = states.shape[1]
    rows = held * steps
    features = depth * ndp
    first_row = lax.axis_index("dp") * held
    held_lengths = lax.dynamic_slice_in_dim(lengths, first_row, held, 0)
    live = jnp.arange(steps, dtype=jnp.int32)[None, :] < held_lengths[:, None]
    live = jnp.broadcast_to(live.astype(F32).reshape(rows, 1), (rows, LANES))
    current = tokens.reshape(seqs * steps, depth)
    weights = (w_recept, w_key, w_value, w_decay, w_rate, w_gate)
    finals = None
    for block in range(BLOCKS):
        proj, total = project(
            block, ntp, ndp, rows, current, norm_gain[block : block + 1], weights, 2 * block
        )
        gated, finals = mix(
            block, features, steps, proj, total, live,
            decay_base[block : block + 1], out_gain[block : block + 1], states, finals,
        )
        current = output(block, ntp, ndp, gated, current, w_out, 2 * block + 1)
    return (current.reshape(seqs, steps, depth), finals)


def solution(mesh):
    in_specs = (
        P(("grp", "tp"), None, "dp"),
        P("grp"),
        P(None, "dp"),
        P(None, "dp", "tp"),
        P(None, "dp", "tp"),
        P(None, "dp", "tp"),
        P(None, "dp", "tp"),
        P(None, "dp", "tp"),
        P(None, "dp", "tp"),
        P(None, "tp", "dp"),
        P(None, "tp"),
        P(None, "tp"),
        P(None, ("grp", "dp"), None, "tp"),
    )
    out_specs = (P(("grp", "tp"), None, "dp"), P(None, ("grp", "dp"), None, "tp"))
    run = functools.partial(body, mesh.shape["tp"], mesh.shape["dp"])
    return jax.shard_map(run, mesh=mesh, in_specs=in_specs, out_specs=out_specs, check_vma=False)
```

profile of v0, /device:TPU:15, one launch (start us, length us, event | category | flops | bytes accessed | tf_op | source)
XLA Modules:
  0.0 131.0 jit_solution(3615094109559551676)
XLA Ops:
  0.6 0.7 dynamic_slice.3
  1.4 0.1 fusion
  1.4 0.1 reshape.31
  1.5 0.8 fusion.2
  2.3 0.8 fusion.1
  3.1 0.1 broadcast_in_dim.2.live_ref
  3.2 0.0 copy-start.2
  3.2 1.6 %copy-done.2 = bf16[2,1024,512]{2,1,0:T(8,128)(2,1)S(1)} copy-done((bf16[2,1024,512]{2,1,0:T(8,128)(2,1)S(1)}, bf16[2,1024,512]{2,1,0:T(8,128)(2,1)}, u32[]{:S(2)}) %copy-start.2) | copy-done | bytes 2097176
  4.8 0.0 copy-start.4
  4.8 1.6 %copy-done.4 = bf16[2,1024,512]{2,1,0:T(8,128)(2,1)S(1)} copy-done((bf16[2,1024,512]{2,1,0:T(8,128)(2,1)S(1)}, bf16[2,1024,512]{2,1,0:T(8,128)(2,1)}, u32[]{:S(2)}) %copy-start.4) | copy-done | bytes 2097176
  6.3 0.0 copy-start.6
  6.4 0.9 copy-done.6
  7.3 0.0 copy-start
  7.3 0.0 copy-start.5
  7.3 30.7 %project0.1 = (f32[64,3072]{1,0:T(8,128)S(1)}, f32[64,128]{1,0:T(8,128)S(1)}) custom-call(bf16[64,1024]{1,0:T(8,128)(2,1)S(1)} %bitcast.3, f32[1,1024]{1,0:T(1,128)S(1)} %get-tuple-element.19.gain_ref, bf16[2,1024,512]{2,1,0:T(8,128)(2,1)S(1)} %copy-done.2, bf16[2,1024,512]{2,1,0:T(8,128)(2,1)S(1)} %copy-done.4, bf16[2,1024,512]{2,1,0:T(8,128)(2,1)} %w2.3, ...), custom_call_target="tpu_custom_call" | custom-call | tf_op jit(solution)/shard_map/project0/pallas_call | solution.py:186
  37.9 0.0 copy-start.1
  37.9 0.0 copy-done
  38.0 0.0 copy-start.3
  38.0 10.5 %mix0.1 = (bf16[64,512]{1,0:T(8,128)(2,1)S(1)}, f32[2,8,64,512]{3,2,1,0:T(8,128)}) custom-call(f32[64,3072]{1,0:T(8,128)S(1)} %get-tuple-element.10.proj_ref, f32[64,128]{1,0:T(8,128)S(1)} %get-tuple-element.11.total_ref, f32[64,128]{1,0:T(8,128)S(1)} %broadcast_in_dim.2.live_ref, f32[1,512]{1,0:T(1,128)S(1)} %get-tuple-element.24.base_ref, ...), custom_call_target="tpu_custom_call" | custom-call | tf_op jit(solution)/shard_map/mix0/pallas_call | solution.py:339
  48.5 0.0 copy-done.1
  48.5 20.5 %output0.1.x_ref = f32[64,1024]{1,0:T(8,128)S(1)} custom-call(bf16[64,512]{1,0:T(8,128)(2,1)S(1)} %get-tuple-element.12.gated_ref, bf16[64,1024]{1,0:T(8,128)(2,1)S(1)} %bitcast.4, bf16[2,512,1024]{2,1,0:T(8,128)(2,1)S(1)} %copy-done.1), custom_call_target="tpu_custom_call" | custom-call | tf_op jit(solution)/shard_map/output0/pallas_call | solution.py:414
  69.0 0.0 copy-done.5
  69.1 0.0 copy-done.3
  69.1 30.2 %project1.1 = (f32[64,3072]{1,0:T(8,128)S(1)}, f32[64,128]{1,0:T(8,128)S(1)}) custom-call(f32[64,1024]{1,0:T(8,128)S(1)} %output0.1.x_ref, f32[1,1024]{1,0:T(1,128)S(1)} %get-tuple-element.18.gain_ref, bf16[2,1024,512]{2,1,0:T(8,128)(2,1)S(1)} %copy-done.3, bf16[2,1024,512]{2,1,0:T(8,128)(2,1)S(1)} %copy-done.5, bf16[2,1024,512]{2,1,0:T(8,128)(2,1)} %w2.3, ...), custom_call_target="tpu_custom_call" | custom-call | tf_op jit(solution)/shard_map/project1/pallas_call | solution.py:186
  99.2 10.5 %mix1.1 = (bf16[64,512]{1,0:T(8,128)(2,1)S(1)}, f32[2,8,64,512]{3,2,1,0:T(8,128)}) custom-call(f32[64,3072]{1,0:T(8,128)S(1)} %get-tuple-element.13.proj_ref, f32[64,128]{1,0:T(8,128)S(1)} %get-tuple-element.14.total_ref, f32[64,128]{1,0:T(8,128)S(1)} %broadcast_in_dim.2.live_ref, ...), custom_call_target="tpu_custom_call", output_to_operand_aliasing={{1}: (6, {})} | custom-call | tf_op jit(solution)/shard_map/mix1/pallas_call | solution.py:339
  109.7 20.5 %output1.1 = f32[64,1024]{1,0:T(8,128)S(1)} custom-call(bf16[64,512]{1,0:T(8,128)(2,1)S(1)} %get-tuple-element.16.gated_ref, f32[64,1024]{1,0:T(8,128)S(1)} %output0.1.x_ref, bf16[2,512,1024]{2,1,0:T(8,128)(2,1)S(1)} %copy-done.1), custom_call_target="tpu_custom_call" | custom-call | tf_op jit(solution)/shard_map/output1/pallas_call | solution.py:414
  130.3 0.7 copy.18
Async XLA Ops:
  3.2 1.6 %copy-start.2 = (bf16[2,1024,512]{2,1,0:T(8,128)(2,1)S(1)}, bf16[2,1024,512]{2,1,0:T(8,128)(2,1)}, u32[]{:S(2)}) copy-start(bf16[2,1024,512]{2,1,0:T(8,128)(2,1)} %w0.3) | copy-start | bytes 6291460
  4.8 1.6 %copy-start.4 = (bf16[2,1024,512]{2,1,0:T(8,128)(2,1)S(1)}, bf16[2,1024,512]{2,1,0:T(8,128)(2,1)}, u32[]{:S(2)}) copy-start(bf16[2,1024,512]{2,1,0:T(8,128)(2,1)} %w1.3) | copy-start | bytes 6291460
  6.3 0.9 copy-start.6
  7.3 30.7 %copy-start = (f32[2,8,64,512]{3,2,1,0:T(8,128)S(1)}, f32[2,8,64,512]{3,2,1,0:T(8,128)}, u32[]{:S(2)}) copy-start(f32[2,8,64,512]{3,2,1,0:T(8,128)} %state_ref.3) | copy-start | bytes 6291460
  7.3 61.8 %copy-start.5 = (bf16[2,1024,512]{2,1,0:T(8,128)(2,1)S(1)}, bf16[2,1024,512]{2,1,0:T(8,128)(2,1)}, u32[]{:S(2)}) copy-start(bf16[2,1024,512]{2,1,0:T(8,128)(2,1)} %w1.3) | copy-start | bytes 6291460
  37.9 10.6 %copy-start.1 = (bf16[2,512,1024]{2,1,0:T(8,128)(2,1)S(1)}, bf16[2,512,1024]{2,1,0:T(8,128)(2,1)}, u32[]{:S(2)}) copy-start(bf16[2,512,1024]{2,1,0:T(8,128)(2,1)} %w_ref.3) | copy-start | bytes 6291460
  38.0 31.1 %copy-start.3 = (bf16[2,1024,512]{2,1,0:T(8,128)(2,1)S(1)}, bf16[2,1024,512]{2,1,0:T(8,128)(2,1)}, u32[]{:S(2)}) copy-start(bf16[2,1024,512]{2,1,0:T(8,128)(2,1)} %w0.3) | copy-start | bytes 6291460
where the time goes:
time: 131 us
  Pallas kernels  123 us (94%)
  local copies, waits for them, and re-layouts  7.26 us (6%)
    pallas_call x2, Pallas kernels, project(): pl.pallas_call(functools.partial(project_kernel, block, ntp, ndp, rows, w...  60.8 us
    pallas_call x2, Pallas kernels, output(): pl.pallas_call(functools.partial(output_kernel, block, ntp, ndp, rows), o...  41.1 us
    pallas_call x2, Pallas kernels, mix(): pl.pallas_call(functools.partial(mix_kernel, features, steps), grid=(1,),...  21 us
    unnamed x15, local copies, waits for them, and re-layouts  4.82 us

commit v1 on v0

v1 whole, which is shorter than its diff:
```python
import functools

import jax
import jax.numpy as jnp
from jax import lax
from jax.experimental import pallas as pl
from jax.experimental.pallas import tpu as pltpu
from jax.sharding import PartitionSpec as P

HEAD = 64
BLOCKS = 2
LANES = 128
CORES = 2

group_eps = 0.00064
norm_eps = 1e-06
key_eps = 1e-06
decay_scale = 0.606531
MESH = pl.DeviceIdType.MESH
F32 = jnp.float32
BF16 = jnp.bfloat16


def remote(src, dst, send, recv, axis, peer):
    return pltpu.make_async_remote_copy(
        src_ref=src,
        dst_ref=dst,
        send_sem=send,
        recv_sem=recv,
        device_id={axis: peer},
        device_id_type=MESH,
    )


def greet(peers):
    barrier = pltpu.get_barrier_semaphore()
    for axis, peer in peers:
        pl.semaphore_signal(barrier, inc=1, device_id={axis: peer}, device_id_type=MESH)
    pl.semaphore_wait(barrier, len(peers))


def grid_of(shape, dim):
    return lax.broadcasted_iota(jnp.int32, shape, dim)


def dot(a, b, dims=(((1,), (0,)), ((), ()))):
    return lax.dot_general(a.astype(BF16), b.astype(BF16), dims, preferred_element_type=F32)


def exact(a, b, dims=(((1,), (0,)), ((), ()))):
    return lax.dot_general(
        a, b, dims, preferred_element_type=F32, precision=lax.Precision.HIGHEST
    )


def split_dot(a, b):
    hi = a.astype(BF16)
    lo = (a - hi.astype(F32)).astype(BF16)
    return jnp.dot(hi, b, preferred_element_type=F32) + jnp.dot(lo, b, preferred_element_type=F32)


NT = (((1,), (1,)), ((), ()))
TN = (((0,), (0,)), ((), ()))


def mix(
    features, steps, block, proj, total, live, base, gain, state, final, span,
    vals_s, seen_s, read_s, ask_s, on_s,
):
    rows = total.shape[0]
    held = rows // steps
    heads = span // HEAD
    tall = steps * heads
    inv = lax.rsqrt(jnp.sum(total, axis=1, keepdims=True) / features + norm_eps)
    recept, keys, values, decay_pre, rate_pre, gate_pre = (proj(i) * inv for i in range(6))
    seg = (grid_of((span, span), 0) // HEAD == grid_of((span, span), 1) // HEAD).astype(F32).astype(BF16)
    unit = keys * lax.rsqrt(split_dot(keys * keys, seg) + key_eps)
    removal = unit * jax.nn.sigmoid(rate_pre) * live
    logd = -decay_scale * jax.nn.sigmoid(decay_pre + base) * live
    step_of = grid_of((rows, 1), 0) % steps
    upto = logd
    shift = 1
    while shift < steps:
        upto = upto + jnp.where(step_of >= shift, pltpu.roll(upto, shift, 0), 0.0)
        shift *= 2
    grow = jnp.exp(upto)
    back = jnp.exp(-upto)
    u_in = unit * jnp.exp(upto - logd)
    q_in = recept * grow
    r_out = removal * back
    k_out = keys * live * back
    scale_out = gain * jax.nn.sigmoid(gate_pre) * live

    lane = grid_of((rows, LANES), 1)
    for j in range(span // LANES):
        pair = values[:, j * LANES : (j + 1) * LANES]
        vals_s[pl.ds(2 * j, rows, stride=heads), :] = pair
        vals_s[pl.ds(2 * j + 1, rows, stride=heads), :] = pltpu.roll(pair, HEAD, 1)

    if heads % 8 == 0:
        one = jnp.where(grid_of((heads, span), 0) == grid_of((heads, span), 1) // HEAD, 1.0, 0.0)

        def spread(a):
            return jnp.concatenate(
                [jnp.broadcast_to(a[s : s + 1], (heads, span)) * one for s in range(steps)], axis=0
            )
    else:
        pick = jnp.where(grid_of((tall, steps), 0) // heads == grid_of((tall, steps), 1), 1.0, 0.0)
        mask = jnp.where(grid_of((tall, span), 0) % heads == grid_of((tall, span), 1) // HEAD, 1.0, 0.0)

        def spread(a):
            return dot(pick, a) * mask

    pad = jnp.zeros((LANES - HEAD - 2 * steps, span), F32)
    ends = []
    for b in range(held):
        cut = slice(b * steps, (b + 1) * steps)
        ask_s[b, 0:tall, :] = spread(u_in[cut]).astype(BF16)
        ask_s[b, tall : 2 * tall, :] = spread(q_in[cut]).astype(BF16)
        ends.append(grow[(b + 1) * steps - 1 : (b + 1) * steps])
    for b in range(held):
        cut = slice(b * steps, (b + 1) * steps)
        against = jnp.concatenate([state[block, b], r_out[cut], k_out[cut], pad], axis=0)
        on_s[b] = dot(ask_s[b], against, NT)

    for b in range(held):
        first = b * tall
        vals = [vals_s[first + s * heads : first + (s + 1) * heads, :] for s in range(steps)]
        seen = []
        for s in range(steps):
            on = on_s[b, s * heads : (s + 1) * heads, :]
            acc = on
            for p in range(s):
                r = on[:, HEAD + p : HEAD + p + 1]
                k = on[:, HEAD + steps + p : HEAD + steps + p + 1]
                acc = acc + (k * vals[p] - r * seen[p])
            seen.append(acc)
            seen_s[first + s * heads : first + (s + 1) * heads, :] = acc
            on = on_s[b, tall + s * heads : tall + (s + 1) * heads, :]
            acc = on
            for p in range(s + 1):
                r = on[:, HEAD + p : HEAD + p + 1]
                k = on[:, HEAD + steps + p : HEAD + steps + p + 1]
                acc = acc + (k * vals[p] - r * seen[p])
            read_s[first + s * heads : first + (s + 1) * heads, :] = acc

    low = grid_of((held * tall, LANES), 1) < HEAD
    read = jnp.where(low, read_s[...], 0.0)
    mean = jnp.sum(read, axis=1, keepdims=True) / HEAD
    centered = jnp.where(low, read - mean, 0.0)
    var = jnp.sum(centered * centered, axis=1, keepdims=True) / HEAD
    read_s[...] = centered * lax.rsqrt(var + group_eps)
    flat = []
    for j in range(span // LANES):
        even = read_s[pl.ds(2 * j, rows, stride=heads), :]
        odd = read_s[pl.ds(2 * j + 1, rows, stride=heads), :]
        flat.append(jnp.where(lane < HEAD, even, pltpu.roll(odd, HEAD, 1)))
    gated = (jnp.concatenate(flat, axis=1) * scale_out).astype(BF16)

    def update():
        for b in range(held):
            cut = slice(b * steps, (b + 1) * steps)
            band = slice(b * tall, (b + 1) * tall)
            left = jnp.concatenate([vals_s[band, :], -seen_s[band, :]], axis=0)
            right = jnp.concatenate(
                [spread(k_out[cut] * ends[b]), spread(r_out[cut] * ends[b])], axis=0
            )
            final[block, b] = state[block, b] * ends[b] + dot(left, right, TN)[0:HEAD]

    return gated, update


def whole_kernel(
    ntp, ndp, steps, features, width,
    tokens, lengths, norm_gain, w0, w1, w2, w3, w4, w5, w_out, base_in, gain_in, states,
    out_ref, final_ref,
    xtok, lens, gains, bases, ogains, wbuf, wobuf, state,
    xg, sqg, part, send_a, recv_a, send_b, recv_b, sq_a, sq_ra, sq_b, sq_rb, totals,
    gg, osend, orecv, current,
    vals_s, seen_s, read_s, ask_s, on_s,
    load_sem, wsem, xs_sem, xr_sem, ss_sem, sr_sem, as_sem, ar_sem, bs_sem, br_sem,
    qas_sem, qar_sem, qbs_sem, qbr_sem, gs_sem, gr_sem, os_sem, or_sem,
):
    weights = (w0, w1, w2, w3, w4, w5)
    _, chunks, depth, _ = wbuf.shape
    halves = chunks // 6
    span = wobuf.shape[1]
    here = xg.shape[2]
    rows = totals.shape[0]
    held = rows // steps
    nx = ndp // CORES
    tp = lax.axis_index("tp")
    dp = lax.axis_index("dp")
    core = lax.rem(dp, CORES)
    xpos = dp // CORES
    partner = dp + 1 - 2 * core

    loads = [
        pltpu.make_async_copy(src, dst, load_sem.at[i])
        for i, (src, dst) in enumerate(
            (
                (tokens, xtok), (norm_gain, gains), (lengths, lens), (base_in, bases),
                (gain_in, ogains), (states, state), (w_out, wobuf),
            )
        )
    ]
    for cp in loads[:5]:
        cp.start()

    def load(block, c):
        return pltpu.make_async_copy(
            weights[c // halves].at[block, :, pl.ds((c % halves) * width, width)],
            wbuf.at[block, c],
            wsem.at[block, c],
        )

    for c in range(chunks):
        load(0, c).start()
    loads[5].start()
    loads[6].start()
    for block in range(1, BLOCKS):
        for c in range(chunks):
            load(block, c).start()
    greet(
        [("tp", lax.rem(tp + k, ntp)) for k in range(1, ntp)]
        + [("dp", lax.rem(dp + k, ndp)) for k in range(1, ndp)]
    )
    for cp in loads[:5]:
        cp.wait()
    current[...] = xtok[...].reshape(here, depth).astype(F32)
    seq_of = grid_of((rows, 1), 0) // steps
    count = jnp.zeros((rows, 1), jnp.int32)
    for b in range(held):
        count = jnp.where(seq_of == b, lens[dp * held + b], count)
    live = jnp.where(grid_of((rows, 1), 0) % steps < count, 1.0, 0.0)

    for block in range(BLOCKS):
        x = current[...]
        xg[block, tp] = (x * gains[block : block + 1, :]).astype(BF16)
        sq = x * x
        acc = sq[:, 0:LANES]
        for k in range(1, depth // LANES):
            acc = acc + sq[:, k * LANES : (k + 1) * LANES]
        sqg[block, tp] = acc

        gathers = []
        for k in range(1, ntp):
            peer = lax.rem(tp + k, ntp)
            cp = remote(
                xg.at[block, tp], xg.at[block, tp], xs_sem.at[block, k], xr_sem.at[block, k], "tp", peer
            )
            cq = remote(
                sqg.at[block, tp], sqg.at[block, tp], ss_sem.at[block, k], sr_sem.at[block, k], "tp", peer
            )
            cp.start()
            cq.start()
            gathers += [cp, cq]
        for k in range(1, ntp):
            src = lax.rem(tp + ntp - k, ntp)
            remote(
                xg.at[block, src], xg.at[block, src], xs_sem.at[block, k], xr_sem.at[block, k], "tp", src
            ).wait_recv()
            remote(
                sqg.at[block, src], sqg.at[block, src], ss_sem.at[block, k], sr_sem.at[block, k], "tp", src
            ).wait_recv()

        sq_all = sqg[block].reshape(ndp, rows, LANES)
        part_sq = [sq_all[d] for d in range(ndp)]

        def pick(parts, x_at, which):
            return jnp.where(which == 0, parts[CORES * x_at], parts[CORES * x_at + 1])

        for xd in range(nx):
            sq_a[block, xd] = pick(part_sq, xd, 1 - core)
            sq_b[block, xd] = pick(part_sq, xd, core)
        copy_qa = remote(
            sq_a.at[block], sq_ra.at[block], qas_sem.at[block], qar_sem.at[block], "dp", partner
        )
        copy_qa.start()

        def copy_a(c):
            return remote(
                send_a.at[block, c], recv_a.at[block, c], as_sem.at[block, c], ar_sem.at[block, c],
                "dp", partner,
            )

        def copy_b(c, k):
            xd = lax.rem(xpos + k, nx)
            return remote(
                send_b.at[block, c, k], recv_b.at[block, c, k],
                bs_sem.at[block, c, k], br_sem.at[block, c, k],
                "dp", CORES * xd + core,
            )

        def stage_b(c):
            copy_a(c).wait_recv()
            for k in range(1, nx):
                xd = lax.rem(xpos + k, nx)
                send_b[block, c, k] = (
                    part[c, CORES * xd + core] + recv_a[block, c, xd].astype(F32)
                ).astype(BF16)
                copy_b(c, k).start()

        def first(c, carry):
            pltpu.make_async_copy(wbuf.at[block, c], wbuf.at[block, c], wsem.at[block, c]).wait()
            res = jnp.dot(
                xg[block].reshape(ndp * rows, depth), wbuf[block, c], preferred_element_type=F32
            )
            part[c] = res.reshape(ndp, rows, width)
            for xd in range(nx):
                send_a[block, c, xd] = part[c, CORES * xd + 1 - core].astype(BF16)
            copy_a(c).start()

            @pl.when(c > 0)
            def _():
                stage_b(c - 1)

            return carry

        lax.fori_loop(0, chunks, first, 0)
        copy_qa.wait_recv()
        for xd in range(nx):
            sq_b[block, xd] = sq_b[block, xd] + sq_ra[block, xd]
        qb = []
        for k in range(1, nx):
            xd = lax.rem(xpos + k, nx)
            cp = remote(
                sq_b.at[block, xd], sq_rb.at[block, k], qbs_sem.at[block, k], qbr_sem.at[block, k],
                "dp", CORES * xd + core,
            )
            cp.start()
            qb.append(cp)
        stage_b(chunks - 1)

        def last(c, carry):
            own = part[c, CORES * xpos + core] + recv_a[block, c, xpos].astype(F32)
            for k in range(1, nx):
                copy_b(c, k).wait_recv()
                own = own + recv_b[block, c, k].astype(F32)
            totals[:, pl.ds(pl.multiple_of(c * width, width), width)] = own
            copy_a(c).wait_send()
            for k in range(1, nx):
                copy_b(c, k).wait_send()
            return carry

        lax.fori_loop(0, chunks, last, 0)
        total = sq_b[block, xpos]
        for k in range(1, nx):
            qb[k - 1].wait_recv()
            total = total + sq_rb[block, k]

        if block == 0:
            loads[5].wait()
            loads[6].wait()
        gated, update = mix(
            features, steps, block, lambda i: totals[:, i * span : (i + 1) * span], total, live,
            bases[block : block + 1, :], ogains[block : block + 1, :], state, final_ref, span,
            vals_s, seen_s, read_s, ask_s, on_s,
        )
        gg[block, dp] = gated
        shares = []
        for k in range(1, ndp):
            cp = remote(
                gg.at[block, dp], gg.at[block, dp], gs_sem.at[block, k], gr_sem.at[block, k],
                "dp", lax.rem(dp + k, ndp),
            )
            cp.start()
            shares.append(cp)
        update()
        for k in range(1, ndp):
            src = lax.rem(dp + ndp - k, ndp)
            remote(
                gg.at[block, src], gg.at[block, src], gs_sem.at[block, k], gr_sem.at[block, k], "dp", src
            ).wait_recv()
        every = gg.at[block].reshape(ntp, here, span)

        def partial_of(peer):
            return jnp.dot(every[peer], wobuf[block], preferred_element_type=F32)

        def copy_o(k):
            return remote(
                osend.at[block, k], orecv.at[block, k], os_sem.at[block, k], or_sem.at[block, k],
                "tp", lax.rem(tp + k, ntp),
            )

        def give(k, carry):
            osend[block, k] = partial_of(lax.rem(tp + k, ntp)).astype(BF16)
            copy_o(k).start()
            return carry

        lax.fori_loop(1, ntp, give, 0)
        current[...] += partial_of(tp)

        def take(k, carry):
            copy_o(k).wait_recv()
            current[...] += orecv[block, k].astype(F32)
            copy_o(k).wait_send()
            return carry

        lax.fori_loop(1, ntp, take, 0)
        copy_qa.wait_send()
        for cp in qb + gathers + shares:
            cp.wait_send()
    out_ref[...] = current[...].reshape(out_ref.shape)


def body(
    ntp, ndp,
    tokens, lengths, norm_gain,
    w_recept, w_key, w_value, w_decay, w_rate, w_gate,
    w_out, decay_base, out_gain, states,
):
    seqs, steps, depth = tokens.shape
    held = states.shape[1]
    rows = held * steps
    here = seqs * steps
    features = depth * ndp
    span = w_key.shape[2]
    width = min(256, span)
    chunks = 6 * span // width
    nx = ndp // CORES
    heads = span // HEAD
    tall = steps * heads
    dma = pltpu.SemaphoreType.DMA
    vmem = pl.BlockSpec(memory_space=pltpu.VMEM)
    hbm = pl.BlockSpec(memory_space=pl.ANY)
    B = BLOCKS

    def buf(*shape, dtype=F32):
        return pltpu.VMEM(shape, dtype)

    return pl.pallas_call(
        functools.partial(whole_kernel, ntp, ndp, steps, features, width),
        out_shape=(
            jax.ShapeDtypeStruct((seqs, steps, depth), F32),
            jax.ShapeDtypeStruct(states.shape, F32),
        ),
        in_specs=[hbm] * 13,
        out_specs=(vmem, vmem),
        scratch_shapes=[
            buf(seqs, steps, depth, dtype=BF16),
            pltpu.SMEM(lengths.shape, jnp.int32),
            buf(B, depth), buf(B, span), buf(B, span),
            buf(B, chunks, depth, width, dtype=BF16),
            buf(B, span, depth, dtype=BF16),
            buf(*states.shape),
            buf(B, ntp, here, depth, dtype=BF16),
            buf(B, ntp, here, LANES),
            buf(chunks, ndp, rows, width),
            buf(B, chunks, nx, rows, width, dtype=BF16),
            buf(B, chunks, nx, rows, width, dtype=BF16),
            buf(B, chunks, nx, rows, width, dtype=BF16),
            buf(B, chunks, nx, rows, width, dtype=BF16),
            buf(B, nx, rows, LANES), buf(B, nx, rows, LANES),
            buf(B, nx, rows, LANES), buf(B, nx, rows, LANES),
            buf(rows, 6 * span),
            buf(B, ndp, rows, span, dtype=BF16),
            buf(B, ntp, here, depth, dtype=BF16),
            buf(B, ntp, here, depth, dtype=BF16),
            buf(here, depth),
            buf(held * tall, LANES), buf(held * tall, LANES), buf(held * tall, LANES),
            buf(held, 2 * tall, span, dtype=BF16), buf(held, 2 * tall, LANES),
            dma((7,)), dma((B, chunks)),
            dma((B, ntp)), dma((B, ntp)), dma((B, ntp)), dma((B, ntp)),
            dma((B, chunks)), dma((B, chunks)),
            dma((B, chunks, nx)), dma((B, chunks, nx)),
            dma((B,)), dma((B,)), dma((B, nx)), dma((B, nx)),
            dma((B, ndp)), dma((B, ndp)), dma((B, ntp)), dma((B, ntp)),
        ],
        compiler_params=pltpu.CompilerParams(
            collective_id=0, has_side_effects=True, vmem_limit_bytes=60 * 1024 * 1024
        ),
        name="whole",
    )(
        tokens, lengths, norm_gain,
        w_recept, w_key, w_value, w_decay, w_rate, w_gate,
        w_out, decay_base, out_gain, states,
    )


def solution(mesh):
    in_specs = (
        P(("grp", "tp"), None, "dp"),
        P("grp"),
        P(None, "dp"),
        P(None, "dp", "tp"),
        P(None, "dp", "tp"),
        P(None, "dp", "tp"),
        P(None, "dp", "tp"),
        P(None, "dp", "tp"),
        P(None, "dp", "tp"),
        P(None, "tp", "dp"),
        P(None, "tp"),
        P(None, "tp"),
        P(None, ("grp", "dp"), None, "tp"),
    )
    out_specs = (P(("grp", "tp"), None, "dp"), P(None, ("grp", "dp"), None, "tp"))
    run = functools.partial(body, mesh.shape["tp"], mesh.shape["dp"])
    return jax.shard_map(run, mesh=mesh, in_specs=in_specs, out_specs=out_specs, check_vma=False)
```

time: 131 us -> 109 us (0.83)
  Pallas kernels: 123 us -> 103 us
  local copies, waits for them, and re-layouts: 7.26 us -> 4.81 us
    pallas_call x6 -> x1, Pallas kernels: 123 us -> 103 us  [body(): pl.pallas_call(functools.partial(whole_kernel, ntp, ndp, steps, features,...]
    slice x2 -> x0, local copies, waits for them, and re-layouts: 1.56 us -> none  [the longest x1 0.78 us: body(): norm_gain[block:block + 1]]
    unnamed x15 -> x2, local copies, waits for them, and re-layouts: 4.82 us -> 4.81 us
where the time goes in v1:
time: 109 us
  Pallas kernels  103 us (94%)
  local copies, waits for them, and re-layouts  4.81 us (4%)
    pallas_call x1, Pallas kernels, body(): pl.pallas_call(functools.partial(whole_kernel, ntp, ndp, steps, features,...  103 us
    unnamed x2, local copies, waits for them, and re-layouts  4.81 us

profile of v1, /device:TPU:15, one launch (start us, length us, event | category | flops | bytes accessed | tf_op | source)
XLA Modules:
  0.0 108.8 jit_solution(2573350704730996177)
XLA Ops:
  0.6 103.3 %whole.1 = (f32[8,8,1024]{2,1,0:T(8,128)}, f32[2,8,64,512]{3,2,1,0:T(8,128)}) custom-call(bf16[8,8,1024]{2,1,0:T(8,128)(2,1)} %tokens.1, s32[32]{0:T(128)} %lengths.1, f32[2,1024]{1,0:T(2,128)} %norm_gain.1, bf16[2,1024,512]{2,1,0:T(8,128)(2,1)} %w0.1, bf16[2,1024,512]{2,1,0:T(8,128)(2,1)} %w1.1, bf16[2,1024,512]{2,1,0:T(8,128)(2,1)} %w2.1, ...), custom_call_target="tpu_custom_call" | custom-call | tf_op jit(solution)/shard_map/whole/pallas_call | solution.py:432
  104.0 1.7 %copy.17 = f32[8,8,1024]{2,1,0:T(8,128)} copy(f32[8,8,1024]{2,1,0:T(8,128)} %get-tuple-element.4) | data formatting | bytes 524288
  105.6 3.1 %copy.18 = f32[2,8,64,512]{3,2,1,0:T(8,128)} copy(f32[2,8,64,512]{3,2,1,0:T(8,128)} %get-tuple-element.5) | data formatting | bytes 4194304

commit v2 on v1

--- a/solution.py
+++ b/solution.py
@@ -59,20 +59,40 @@
     return jnp.dot(hi, b, preferred_element_type=F32) + jnp.dot(lo, b, preferred_element_type=F32)
 
 
+def split_right(a, b):
+    hi = b.astype(BF16)
+    lo = (b - hi.astype(F32)).astype(BF16)
+    return jnp.dot(a, hi, preferred_element_type=F32) + jnp.dot(a, lo, preferred_element_type=F32)
+
+
+def by_index(values, index):
+    out = jnp.full(index.shape, values[0], jnp.int32)
+    for i in range(1, len(values)):
+        out = jnp.where(index == i, values[i], out)
+    return out
+
+
+def lane_sums(x):
+    sq = x * x
+    acc = sq[:, 0:LANES]
+    for k in range(1, x.shape[1] // LANES):
+        acc = acc + sq[:, k * LANES : (k + 1) * LANES]
+    return acc
+
+
 NT = (((1,), (1,)), ((), ()))
 TN = (((0,), (0,)), ((), ()))
 
 
 def mix(
-    features, steps, block, proj, total, live, base, gain, state, final, span,
+    steps, block, projected, live, base, gain, state, final, span,
     vals_s, seen_s, read_s, ask_s, on_s,
 ):
-    rows = total.shape[0]
+    recept, keys, values, decay_pre, rate_pre, gate_pre = projected
+    rows = recept.shape[0]
     held = rows // steps
     heads = span // HEAD
     tall = steps * heads
-    inv = lax.rsqrt(jnp.sum(total, axis=1, keepdims=True) / features + norm_eps)
-    recept, keys, values, decay_pre, rate_pre, gate_pre = (proj(i) * inv for i in range(6))
     seg = (grid_of((span, span), 0) // HEAD == grid_of((span, span), 1) // HEAD).astype(F32).astype(BF16)
     unit = keys * lax.rsqrt(split_dot(keys * keys, seg) + key_eps)
     removal = unit * jax.nn.sigmoid(rate_pre) * live
@@ -171,23 +191,28 @@
 
 
 def whole_kernel(
-    ntp, ndp, steps, features, width,
+    ntp, ndp, steps, features, width, cap, share,
     tokens, lengths, norm_gain, w0, w1, w2, w3, w4, w5, w_out, base_in, gain_in, states,
     out_ref, final_ref,
     xtok, lens, gains, bases, ogains, wbuf, wobuf, state,
-    xg, sqg, part, send_a, recv_a, send_b, recv_b, sq_a, sq_ra, sq_b, sq_rb, totals,
-    gg, osend, orecv, current,
+    xg, xpk, sqpk, sqd, accpk, packer, unpacker, xall, part,
+    send_a, recv_a, send_b, recv_b, totals,
+    gg, osend, orecv, psend, precv,
     vals_s, seen_s, read_s, ask_s, on_s,
     load_sem, wsem, xs_sem, xr_sem, ss_sem, sr_sem, as_sem, ar_sem, bs_sem, br_sem,
-    qas_sem, qar_sem, qbs_sem, qbr_sem, gs_sem, gr_sem, os_sem, or_sem,
+    qs_sem, qr_sem, gs_sem, gr_sem, os_sem, or_sem,
 ):
     weights = (w0, w1, w2, w3, w4, w5)
     _, chunks, depth, _ = wbuf.shape
     halves = chunks // 6
     span = wobuf.shape[1]
-    here = xg.shape[2]
     rows = totals.shape[0]
-    held = rows // steps
+    held = state.shape[1]
+    seqs = xtok.shape[0]
+    natural = held * steps
+    here = seqs * steps
+    every = ntp * cap
+    packed = ntp * share
     nx = ndp // CORES
     tp = lax.axis_index("tp")
     dp = lax.axis_index("dp")
@@ -199,7 +224,7 @@
         pltpu.make_async_copy(src, dst, load_sem.at[i])
         for i, (src, dst) in enumerate(
             (
-                (tokens, xtok), (norm_gain, gains), (lengths, lens), (base_in, bases),
+                (tokens, xtok), (lengths, lens), (norm_gain, gains), (base_in, bases),
                 (gain_in, ogains), (states, state), (w_out, wobuf),
             )
         )
@@ -225,58 +250,103 @@
         [("tp", lax.rem(tp + k, ntp)) for k in range(1, ntp)]
         + [("dp", lax.rem(dp + k, ndp)) for k in range(1, ndp)]
     )
-    for cp in loads[:5]:
+    for cp in loads[:2]:
         cp.wait()
-    current[...] = xtok[...].reshape(here, depth).astype(F32)
-    seq_of = grid_of((rows, 1), 0) // steps
-    count = jnp.zeros((rows, 1), jnp.int32)
-    for b in range(held):
-        count = jnp.where(seq_of == b, lens[dp * held + b], count)
-    live = jnp.where(grid_of((rows, 1), 0) % steps < count, 1.0, 0.0)
+
+    def spot(first, number):
+        index = grid_of((number * steps, 1), 0)
+        at, starts, counts = jnp.int32(0), [], []
+        for b in range(number):
+            if b % seqs == 0:
+                at = jnp.int32(b // seqs * cap)
+            starts.append(at)
+            counts.append(lens[first + b])
+            at = at + counts[-1]
+        step = index % steps
+        place = by_index(starts, index // steps) + step
+        alive = step < by_index(counts, index // steps)
+        wide = (number * steps, number // seqs * cap)
+        one = jnp.where((place == grid_of(wide, 1)) & alive, 1.0, 0.0)
+        return one, jnp.where(alive, 1.0, 0.0)
+
+    mine, mine_live = spot(tp * seqs, seqs)
+    mine = mine.astype(BF16)
+    flat_tokens = xtok[...].reshape(here, depth)
+    xg[tp] = dot(mine, flat_tokens, TN).astype(BF16)
+    sends = []
+
+    def gather(buf, k, send, recv):
+        cp = remote(buf.at[tp], buf.at[tp], send.at[k], recv.at[k], "tp", lax.rem(tp + k, ntp))
+        cp.start()
+        sends.append(cp)
+
+    def gathered(buf, k, send, recv):
+        src = lax.rem(tp + ntp - k, ntp)
+        remote(buf.at[src], buf.at[src], send.at[k], recv.at[k], "tp", src).wait_recv()
+
+    for k in range(1, ntp):
+        gather(xg, k, xs_sem.at[0], xr_sem.at[0])
+
+    own_spot, live = spot(dp * held, held)
+    own_spot = own_spot.astype(BF16)
+    starts, counts, at = [], [], jnp.int32(0)
+    for g in range(ntp):
+        starts.append(at)
+        number = jnp.int32(0)
+        for b in range(seqs):
+            number = number + lens[g * seqs + b]
+        counts.append(number)
+        at = at + number
+
+    def ranks(index):
+        return jnp.where(
+            index % cap < by_index(counts, index // cap),
+            by_index(starts, index // cap) + index % cap,
+            -1,
+        )
+
+    packer[...] = jnp.where(
+        grid_of((packed, every), 0) == ranks(grid_of((1, every), 1)), 1.0, 0.0
+    )
+    unpacker[...] = jnp.where(
+        ranks(grid_of((every, 1), 0)) == grid_of((every, packed), 1), 1.0, 0.0
+    ).astype(BF16)
+    accpk[...] = jnp.zeros_like(accpk)
+    own_lanes = jnp.where(
+        grid_of((rows, every), 1) == grid_of((rows, every), 0) + dp * rows, 1.0, 0.0
+    )
+    ones = jnp.ones((8, LANES), F32)
+    for cp in loads[2:5]:
+        cp.wait()
+    for k in range(1, ntp):
+        gathered(xg, k, xs_sem.at[0], xr_sem.at[0])
+    part_rows = pl.ds(pl.multiple_of(tp * share, share), share)
+    current = None
 
     for block in range(BLOCKS):
-        x = current[...]
-        xg[block, tp] = (x * gains[block : block + 1, :]).astype(BF16)
-        sq = x * x
-        acc = sq[:, 0:LANES]
-        for k in range(1, depth // LANES):
-            acc = acc + sq[:, k * LANES : (k + 1) * LANES]
-        sqg[block, tp] = acc
-
-        gathers = []
-        for k in range(1, ntp):
-            peer = lax.rem(tp + k, ntp)
+        if block == 0:
+            x = xg[...].reshape(every, depth).astype(F32)
+            xall[...] = (x * gains[0:1, :]).astype(BF16)
+            sqd[block, dp] = exact(ones, lane_sums(x), NT)
+        else:
+            xpk[tp] = (current * gains[block : block + 1, :]).astype(BF16)
+            accpk[part_rows, :] = lane_sums(current)
+            sqpk[tp] = exact(ones, accpk[...], NT)
+            for k in range(1, ntp):
+                gather(xpk, k, xs_sem.at[1], xr_sem.at[1])
+                gather(sqpk, k, ss_sem, sr_sem)
+            for k in range(1, ntp):
+                gathered(sqpk, k, ss_sem, sr_sem)
+                gathered(xpk, k, xs_sem.at[1], xr_sem.at[1])
+            xall[...] = dot(unpacker[...], xpk[...].reshape(packed, depth)).astype(BF16)
+            sqd[block, dp] = exact(jnp.sum(sqpk[...], axis=0), packer[...])
+        for k in range(1, ndp):
             cp = remote(
-                xg.at[block, tp], xg.at[block, tp], xs_sem.at[block, k], xr_sem.at[block, k], "tp", peer
-            )
-            cq = remote(
-                sqg.at[block, tp], sqg.at[block, tp], ss_sem.at[block, k], sr_sem.at[block, k], "tp", peer
+                sqd.at[block, dp], sqd.at[block, dp], qs_sem.at[block, k], qr_sem.at[block, k],
+                "dp", lax.rem(dp + k, ndp),
             )
             cp.start()
-            cq.start()
-            gathers += [cp, cq]
-        for k in range(1, ntp):
-            src = lax.rem(tp + ntp - k, ntp)
-            remote(
-                xg.at[block, src], xg.at[block, src], xs_sem.at[block, k], xr_sem.at[block, k], "tp", src
-            ).wait_recv()
-            remote(
-                sqg.at[block, src], sqg.at[block, src], ss_sem.at[block, k], sr_sem.at[block, k], "tp", src
-            ).wait_recv()
-
-        sq_all = sqg[block].reshape(ndp, rows, LANES)
-        part_sq = [sq_all[d] for d in range(ndp)]
-
-        def pick(parts, x_at, which):
-            return jnp.where(which == 0, parts[CORES * x_at], parts[CORES * x_at + 1])
-
-        for xd in range(nx):
-            sq_a[block, xd] = pick(part_sq, xd, 1 - core)
-            sq_b[block, xd] = pick(part_sq, xd, core)
-        copy_qa = remote(
-            sq_a.at[block], sq_ra.at[block], qas_sem.at[block], qar_sem.at[block], "dp", partner
-        )
-        copy_qa.start()
+            sends.append(cp)
 
         def copy_a(c):
             return remote(
@@ -303,9 +373,7 @@
 
         def first(c, carry):
             pltpu.make_async_copy(wbuf.at[block, c], wbuf.at[block, c], wsem.at[block, c]).wait()
-            res = jnp.dot(
-                xg[block].reshape(ndp * rows, depth), wbuf[block, c], preferred_element_type=F32
-            )
+            res = jnp.dot(xall[...], wbuf[block, c], preferred_element_type=F32)
             part[c] = res.reshape(ndp, rows, width)
             for xd in range(nx):
                 send_a[block, c, xd] = part[c, CORES * xd + 1 - core].astype(BF16)
@@ -318,90 +386,89 @@
             return carry
 
         lax.fori_loop(0, chunks, first, 0)
-        copy_qa.wait_recv()
-        for xd in range(nx):
-            sq_b[block, xd] = sq_b[block, xd] + sq_ra[block, xd]
-        qb = []
-        for k in range(1, nx):
-            xd = lax.rem(xpos + k, nx)
-            cp = remote(
-                sq_b.at[block, xd], sq_rb.at[block, k], qbs_sem.at[block, k], qbr_sem.at[block, k],
-                "dp", CORES * xd + core,
-            )
-            cp.start()
-            qb.append(cp)
         stage_b(chunks - 1)
+        for k in range(1, ndp):
+            src = lax.rem(dp + ndp - k, ndp)
+            remote(
+                sqd.at[block, src], sqd.at[block, src], qs_sem.at[block, k], qr_sem.at[block, k],
+                "dp", src,
+            ).wait_recv()
+        total = exact(own_lanes, jnp.sum(sqd[block], axis=0), NT)[:, 0:1]
+        inv = lax.rsqrt(total / features + norm_eps)
 
         def last(c, carry):
             own = part[c, CORES * xpos + core] + recv_a[block, c, xpos].astype(F32)
             for k in range(1, nx):
                 copy_b(c, k).wait_recv()
                 own = own + recv_b[block, c, k].astype(F32)
-            totals[:, pl.ds(pl.multiple_of(c * width, width), width)] = own
+            totals[:, pl.ds(pl.multiple_of(c * width, width), width)] = own * inv
             copy_a(c).wait_send()
             for k in range(1, nx):
                 copy_b(c, k).wait_send()
             return carry
 
         lax.fori_loop(0, chunks, last, 0)
-        total = sq_b[block, xpos]
-        for k in range(1, nx):
-            qb[k - 1].wait_recv()
-            total = total + sq_rb[block, k]
-
         if block == 0:
             loads[5].wait()
             loads[6].wait()
         gated, update = mix(
-            features, steps, block, lambda i: totals[:, i * span : (i + 1) * span], total, live,
-            bases[block : block + 1, :], ogains[block : block + 1, :], state, final_ref, span,
+            steps, block,
+            [split_right(own_spot, totals[:, i * span : (i + 1) * span]) for i in range(6)],
+            live, bases[block : block + 1, :], ogains[block : block + 1, :], state, final_ref, span,
             vals_s, seen_s, read_s, ask_s, on_s,
         )
-        gg[block, dp] = gated
-        shares = []
+        gg[block, dp] = dot(own_spot, gated, TN).astype(BF16)
         for k in range(1, ndp):
             cp = remote(
                 gg.at[block, dp], gg.at[block, dp], gs_sem.at[block, k], gr_sem.at[block, k],
                 "dp", lax.rem(dp + k, ndp),
             )
             cp.start()
-            shares.append(cp)
+            sends.append(cp)
         update()
+        if block + 1 < BLOCKS:
+            current = dot(packer[part_rows, :], xg[...].reshape(every, depth))
+        else:
+            back = dot(
+                unpacker[pl.ds(pl.multiple_of(tp * cap, cap), cap), :],
+                xpk[...].reshape(packed, depth),
+            )
+            current = back / gains[block : block + 1, :]
         for k in range(1, ndp):
             src = lax.rem(dp + ndp - k, ndp)
             remote(
                 gg.at[block, src], gg.at[block, src], gs_sem.at[block, k], gr_sem.at[block, k], "dp", src
             ).wait_recv()
-        every = gg.at[block].reshape(ntp, here, span)
-
-        def partial_of(peer):
-            return jnp.dot(every[peer], wobuf[block], preferred_element_type=F32)
-
-        def copy_o(k):
-            return remote(
-                osend.at[block, k], orecv.at[block, k], os_sem.at[block, k], or_sem.at[block, k],
-                "tp", lax.rem(tp + k, ntp),
-            )
-
-        def give(k, carry):
-            osend[block, k] = partial_of(lax.rem(tp + k, ntp)).astype(BF16)
-            copy_o(k).start()
-            return carry
-
-        lax.fori_loop(1, ntp, give, 0)
-        current[...] += partial_of(tp)
-
-        def take(k, carry):
-            copy_o(k).wait_recv()
-            current[...] += orecv[block, k].astype(F32)
-            copy_o(k).wait_send()
-            return carry
-
-        lax.fori_loop(1, ntp, take, 0)
-        copy_qa.wait_send()
-        for cp in qb + gathers + shares:
-            cp.wait_send()
-    out_ref[...] = current[...].reshape(out_ref.shape)
+        rest = gg[block].reshape(every, span)
+        if block + 1 < BLOCKS:
+            rest = dot(packer[...], rest).astype(BF16)
+            sbuf, rbuf = psend, precv
+        else:
+            sbuf, rbuf = osend, orecv
+        size = sbuf.shape[1]
+        partial = jnp.dot(rest, wobuf[block], preferred_element_type=F32)
+        for g in range(ntp):
+            sbuf[g] = partial[g * size : (g + 1) * size].astype(BF16)
+        back_sends = []
+        for k in range(1, ntp):
+            peer = lax.rem(tp + k, ntp)
+            cp = remote(
+                sbuf.at[peer], rbuf.at[k], os_sem.at[block, k], or_sem.at[block, k], "tp", peer
+            )
+            cp.start()
+            sends.append(cp)
+            back_sends.append(cp)
+        for g in range(ntp):
+            current = current + jnp.where(tp == g, partial[g * size : (g + 1) * size], 0.0)
+        for k in range(1, ntp):
+            back_sends[k - 1].wait_recv()
+            current = current + rbuf[k].astype(F32)
+    result = jnp.where(
+        mine_live > 0, exact(mine.astype(F32), current), flat_tokens.astype(F32)
+    )
+    out_ref[...] = result.reshape(out_ref.shape)
+    for cp in sends:
+        cp.wait_send()
 
 
 def body(
@@ -412,8 +479,10 @@
 ):
     seqs, steps, depth = tokens.shape
     held = states.shape[1]
-    rows = held * steps
-    here = seqs * steps
+    live_rows = 7 * lengths.shape[0] // 2
+    cap = seqs * steps
+    share = 16 * -(-live_rows // (16 * ntp))
+    rows = ntp // ndp * cap
     features = depth * ndp
     span = w_key.shape[2]
     width = min(256, span)
@@ -421,6 +490,8 @@
     nx = ndp // CORES
     heads = span // HEAD
     tall = steps * heads
+    every = ntp * cap
+    packed = ntp * share
     dma = pltpu.SemaphoreType.DMA
     vmem = pl.BlockSpec(memory_space=pltpu.VMEM)
     hbm = pl.BlockSpec(memory_space=pl.ANY)
@@ -430,7 +501,7 @@
         return pltpu.VMEM(shape, dtype)
 
     return pl.pallas_call(
-        functools.partial(whole_kernel, ntp, ndp, steps, features, width),
+        functools.partial(whole_kernel, ntp, ndp, steps, features, width, cap, share),
         out_shape=(
             jax.ShapeDtypeStruct((seqs, steps, depth), F32),
             jax.ShapeDtypeStruct(states.shape, F32),
@@ -444,27 +515,31 @@
             buf(B, chunks, depth, width, dtype=BF16),
             buf(B, span, depth, dtype=BF16),
             buf(*states.shape),
-            buf(B, ntp, here, depth, dtype=BF16),
-            buf(B, ntp, here, LANES),
+            buf(ntp, cap, depth, dtype=BF16),
+            buf(ntp, share, depth, dtype=BF16),
+            buf(ntp, 8, packed),
+            buf(B, ndp, 8, every),
+            buf(packed, LANES),
+            buf(packed, every), buf(every, packed, dtype=BF16),
+            buf(every, depth, dtype=BF16),
             buf(chunks, ndp, rows, width),
             buf(B, chunks, nx, rows, width, dtype=BF16),
             buf(B, chunks, nx, rows, width, dtype=BF16),
             buf(B, chunks, nx, rows, width, dtype=BF16),
             buf(B, chunks, nx, rows, width, dtype=BF16),
-            buf(B, nx, rows, LANES), buf(B, nx, rows, LANES),
-            buf(B, nx, rows, LANES), buf(B, nx, rows, LANES),
             buf(rows, 6 * span),
             buf(B, ndp, rows, span, dtype=BF16),
-            buf(B, ntp, here, depth, dtype=BF16),
-            buf(B, ntp, here, depth, dtype=BF16),
-            buf(here, depth),
+            buf(ntp, cap, depth, dtype=BF16),
+            buf(ntp, cap, depth, dtype=BF16),
+            buf(ntp, share, depth, dtype=BF16),
+            buf(ntp, share, depth, dtype=BF16),
             buf(held * tall, LANES), buf(held * tall, LANES), buf(held * tall, LANES),
             buf(held, 2 * tall, span, dtype=BF16), buf(held, 2 * tall, LANES),
             dma((7,)), dma((B, chunks)),
-            dma((B, ntp)), dma((B, ntp)), dma((B, ntp)), dma((B, ntp)),
+            dma((2, ntp)), dma((2, ntp)), dma((ntp,)), dma((ntp,)),
             dma((B, chunks)), dma((B, chunks)),
             dma((B, chunks, nx)), dma((B, chunks, nx)),
-            dma((B,)), dma((B,)), dma((B, nx)), dma((B, nx)),
+            dma((B, ndp)), dma((B, ndp)),
             dma((B, ndp)), dma((B, ndp)), dma((B, ntp)), dma((B, ntp)),
         ],
         compiler_params=pltpu.CompilerParams(

time: 109 us -> 94.5 us (0.87)
  Pallas kernels: 103 us -> 88.9 us
    pallas_call x1, Pallas kernels: 103 us -> 88.9 us  [body(): pl.pallas_call(functools.partial(whole_kernel, ntp, ndp, steps, features,...]
where the time goes in v2:
time: 94.5 us; the launch traced here: 94.4 us
  Pallas kernels  88.9 us (94%)
  local copies, waits for them, and re-layouts  4.81 us (5%)
    pallas_call x1, Pallas kernels, body(): pl.pallas_call(functools.partial(whole_kernel, ntp, ndp, steps, features,...  88.9 us
    unnamed x2, local copies, waits for them, and re-layouts  4.81 us

profile of v2, /device:TPU:15, one launch (start us, length us, event | category | flops | bytes accessed | tf_op | source)
XLA Modules:
  0.0 94.4 jit_solution(16531016701800865513)
XLA Ops:
  0.6 88.9 %whole.1 = (f32[8,8,1024]{2,1,0:T(8,128)}, f32[2,8,64,512]{3,2,1,0:T(8,128)}) custom-call(bf16[8,8,1024]{2,1,0:T(8,128)(2,1)} %tokens.1, s32[32]{0:T(128)} %lengths.1, f32[2,1024]{1,0:T(2,128)} %norm_gain.1, bf16[2,1024,512]{2,1,0:T(8,128)(2,1)} %w0.1, bf16[2,1024,512]{2,1,0:T(8,128)(2,1)} %w1.1, bf16[2,1024,512]{2,1,0:T(8,128)(2,1)} %w2.1, ...), custom_call_target="tpu_custom_call" | custom-call | tf_op jit(solution)/shard_map/whole/pallas_call | solution.py:503
  89.5 1.7 %copy.17 = f32[8,8,1024]{2,1,0:T(8,128)} copy(f32[8,8,1024]{2,1,0:T(8,128)} %get-tuple-element.4) | data formatting | bytes 524288
  91.2 3.1 %copy.18 = f32[2,8,64,512]{3,2,1,0:T(8,128)} copy(f32[2,8,64,512]{3,2,1,0:T(8,128)} %get-tuple-element.5) | data formatting | bytes 4194304

commit v3 on v2

--- a/solution.py
+++ b/solution.py
@@ -190,30 +190,36 @@
     return gated, update
 
 
+def near_first(ntp):
+    rows = [sorted(range(ntp), key=lambda g: (abs(g - t), g)) for t in range(ntp)]
+    return [[rows[t][i] for t in range(ntp)] for i in range(ntp)]
+
+
 def whole_kernel(
-    ntp, ndp, steps, features, width, cap, share,
+    ntp, ndp, steps, features, cap, share, lag,
     tokens, lengths, norm_gain, w0, w1, w2, w3, w4, w5, w_out, base_in, gain_in, states,
     out_ref, final_ref,
     xtok, lens, gains, bases, ogains, wbuf, wobuf, state,
-    xg, xpk, sqpk, sqd, accpk, packer, unpacker, xall, part,
-    send_a, recv_a, send_b, recv_b, totals,
+    xg, xpk, xs, sqpk, sqd0, sqd1, acc0, acc1, packer, unpacker,
+    part0, part1, recv_a0, recv_a1, send_b0, send_b1, recv_b0, recv_b1, tot0, tot1,
     gg, osend, orecv, psend, precv,
     vals_s, seen_s, read_s, ask_s, on_s,
-    load_sem, wsem, xs_sem, xr_sem, ss_sem, sr_sem, as_sem, ar_sem, bs_sem, br_sem,
+    load_sem, wsem, xs_sem, xr_sem, ss_sem, sr_sem, as_sem, ar_sem, bs_sem, br_sem, ds_sem, dr_sem,
     qs_sem, qr_sem, gs_sem, gr_sem, os_sem, or_sem,
 ):
     weights = (w0, w1, w2, w3, w4, w5)
-    _, chunks, depth, _ = wbuf.shape
-    halves = chunks // 6
+    depth = wbuf.shape[2]
     span = wobuf.shape[1]
-    rows = totals.shape[0]
+    pieces, rows, wide = tot0.shape
+    each = wide // span
     held = state.shape[1]
     seqs = xtok.shape[0]
-    natural = held * steps
+    ratio = ntp // ndp
     here = seqs * steps
     every = ntp * cap
     packed = ntp * share
     nx = ndp // CORES
+    count = ntp * pieces
     tp = lax.axis_index("tp")
     dp = lax.axis_index("dp")
     core = lax.rem(dp, CORES)
@@ -233,18 +239,14 @@
         cp.start()
 
     def load(block, c):
-        return pltpu.make_async_copy(
-            weights[c // halves].at[block, :, pl.ds((c % halves) * width, width)],
-            wbuf.at[block, c],
-            wsem.at[block, c],
-        )
-
-    for c in range(chunks):
+        return pltpu.make_async_copy(weights[c].at[block], wbuf.at[block, c], wsem.at[block, c])
+
+    for c in range(6):
         load(0, c).start()
     loads[5].start()
     loads[6].start()
     for block in range(1, BLOCKS):
-        for c in range(chunks):
+        for c in range(6):
             load(block, c).start()
     greet(
         [("tp", lax.rem(tp + k, ntp)) for k in range(1, ntp)]
@@ -265,8 +267,8 @@
         step = index % steps
         place = by_index(starts, index // steps) + step
         alive = step < by_index(counts, index // steps)
-        wide = (number * steps, number // seqs * cap)
-        one = jnp.where((place == grid_of(wide, 1)) & alive, 1.0, 0.0)
+        shape = (number * steps, number // seqs * cap)
+        one = jnp.where((place == grid_of(shape, 1)) & alive, 1.0, 0.0)
         return one, jnp.where(alive, 1.0, 0.0)
 
     mine, mine_live = spot(tp * seqs, seqs)
@@ -275,17 +277,28 @@
     xg[tp] = dot(mine, flat_tokens, TN).astype(BF16)
     sends = []
 
-    def gather(buf, k, send, recv):
-        cp = remote(buf.at[tp], buf.at[tp], send.at[k], recv.at[k], "tp", lax.rem(tp + k, ntp))
-        cp.start()
-        sends.append(cp)
-
-    def gathered(buf, k, send, recv):
-        src = lax.rem(tp + ntp - k, ntp)
-        remote(buf.at[src], buf.at[src], send.at[k], recv.at[k], "tp", src).wait_recv()
-
-    for k in range(1, ntp):
-        gather(xg, k, xs_sem.at[0], xr_sem.at[0])
+    order = near_first(ntp)
+
+    def source(i):
+        at = order[0][0] * 0
+        for k in range(ntp):
+            here_k = order[k][ntp - 1]
+            for t in range(ntp - 1):
+                here_k = jnp.where(tp == t, order[k][t], here_k)
+            at = jnp.where(i == k, here_k, at)
+        return at
+
+    def spread_out(buf, send, recv):
+        for k in range(1, ntp):
+            peer = source(k)
+            cp = remote(buf.at[tp], buf.at[tp], send.at[k], recv.at[tp], "tp", peer)
+            cp.start()
+            sends.append(cp)
+
+    def arrived(buf, send, recv, g):
+        remote(buf.at[g], buf.at[g], send.at[0], recv.at[g], "tp", g).wait_recv()
+
+    spread_out(xg, xs_sem.at[0], xr_sem.at[0])
 
     own_spot, live = spot(dp * held, held)
     own_spot = own_spot.astype(BF16)
@@ -307,113 +320,209 @@
 
     packer[...] = jnp.where(
         grid_of((packed, every), 0) == ranks(grid_of((1, every), 1)), 1.0, 0.0
-    )
+    ).astype(BF16)
     unpacker[...] = jnp.where(
         ranks(grid_of((every, 1), 0)) == grid_of((every, packed), 1), 1.0, 0.0
     ).astype(BF16)
-    accpk[...] = jnp.zeros_like(accpk)
-    own_lanes = jnp.where(
-        grid_of((rows, every), 1) == grid_of((rows, every), 0) + dp * rows, 1.0, 0.0
-    )
+    acc1[...] = jnp.zeros_like(acc1)
     ones = jnp.ones((8, LANES), F32)
     for cp in loads[2:5]:
         cp.wait()
-    for k in range(1, ntp):
-        gathered(xg, k, xs_sem.at[0], xr_sem.at[0])
-    part_rows = pl.ds(pl.multiple_of(tp * share, share), share)
+    mine_packed = pl.ds(pl.multiple_of(tp * share, share), share)
+    own_groups = pl.ds(pl.multiple_of(dp * rows, rows), rows)
     current = None
 
     for block in range(BLOCKS):
-        if block == 0:
-            x = xg[...].reshape(every, depth).astype(F32)
-            xall[...] = (x * gains[0:1, :]).astype(BF16)
-            sqd[block, dp] = exact(ones, lane_sums(x), NT)
+        first_block = block == 0
+        size = cap if first_block else share
+        half = size // CORES
+        part, recv_a, send_b, recv_b, tot, sqd = (
+            (part0, recv_a0, send_b0, recv_b0, tot0, sqd0)
+            if first_block
+            else (part1, recv_a1, send_b1, recv_b1, tot1, sqd1)
+        )
+        my_half = pl.ds(pl.multiple_of(core * half, half), half)
+        other_half = pl.ds(pl.multiple_of((1 - core) * half, half), half)
+        if not first_block:
+            xpk[tp] = (current * gains[block : block + 1, :]).astype(BF16)
+            spread_out(xpk, xs_sem.at[1], xr_sem.at[1])
+            acc1[mine_packed, :] = lane_sums(current)
+            sqpk[tp] = exact(ones, acc1[...], NT)
+            spread_out(sqpk, ss_sem, sr_sem)
+
+        def chip_of(g):
+            return g // ratio // CORES
+
+        def copy_a(g, j):
+            return remote(
+                part.at[g, j, other_half, :], recv_a.at[g, j],
+                as_sem.at[block, g * pieces + j], ar_sem.at[block, g * pieces + j], "dp", partner,
+            )
+
+        def copy_b(g, j, peer, me):
+            return remote(
+                send_b.at[g, j], recv_b.at[me, g, j],
+                bs_sem.at[block, peer, g * pieces + j], br_sem.at[block, me, g * pieces + j],
+                "dp", CORES * peer + core,
+            )
+
+        def copy_d(g, j):
+            base = g * size if not first_block else lax.rem(g, ratio) * size
+            at = tot.at[j, pl.ds(pl.multiple_of(base + core * half, half), half), :]
+            return remote(
+                at, at, ds_sem.at[block, g * pieces + j], dr_sem.at[block, g * pieces + j],
+                "dp", partner,
+            )
+
+        def expect_d(g, j):
+            base = g * size if not first_block else lax.rem(g, ratio) * size
+            at = tot.at[j, pl.ds(pl.multiple_of(base + (1 - core) * half, half), half), :]
+            remote(
+                at, at, ds_sem.at[block, g * pieces + j], dr_sem.at[block, g * pieces + j],
+                "dp", partner,
+            ).wait_recv()
+
+        def stage_b(n):
+            g, j = source(n // pieces), lax.rem(n, pieces)
+            copy_a(g, j).wait_recv()
+            total = part[g, j, my_half, :] + recv_a[g, j]
+            part[g, j, my_half, :] = total
+            send_b[g, j] = total.astype(BF16)
+            for k in range(1, nx):
+                peer = lax.rem(xpos + k, nx)
+                if first_block:
+                    @pl.when(chip_of(g) == peer)
+                    def _():
+                        copy_b(g, j, peer, xpos).start()
+                else:
+                    copy_b(g, j, peer, xpos).start()
+
+        def stage_a(n, carry):
+            g, j = source(n // pieces), lax.rem(n, pieces)
+
+            @pl.when(j == 0)
+            def _():
+                @pl.when(n > 0)
+                def _():
+                    if first_block:
+                        arrived(xg, xs_sem.at[0], xr_sem.at[0], g)
+                    else:
+                        arrived(xpk, xs_sem.at[1], xr_sem.at[1], g)
+
+                if first_block:
+                    x = xg[g].astype(F32)
+                    xs[...] = (x * gains[0:1, :]).astype(BF16)
+                    acc0[pl.ds(pl.multiple_of(g * cap, cap), cap), :] = lane_sums(x)
+
+            @pl.when(n < pieces)
+            def _():
+                for c in range(each):
+                    pltpu.make_async_copy(
+                        wbuf.at[block, j * each + c], wbuf.at[block, j * each + c],
+                        wsem.at[block, j * each + c],
+                    ).wait()
+
+            left = xs[...] if first_block else xpk[g]
+            for c in range(each):
+                part[g, j, :, c * span : (c + 1) * span] = jnp.dot(
+                    left, wbuf[block, j * each + c], preferred_element_type=F32
+                )
+            copy_a(g, j).start()
+
+            @pl.when(n >= lag)
+            def _():
+                stage_b(n - lag)
+
+            return carry
+
+        lax.fori_loop(0, count, stage_a, 0)
+        if first_block:
+            sqd[dp] = exact(ones, acc0[...], NT)
         else:
-            xpk[tp] = (current * gains[block : block + 1, :]).astype(BF16)
-            accpk[part_rows, :] = lane_sums(current)
-            sqpk[tp] = exact(ones, accpk[...], NT)
             for k in range(1, ntp):
-                gather(xpk, k, xs_sem.at[1], xr_sem.at[1])
-                gather(sqpk, k, ss_sem, sr_sem)
-            for k in range(1, ntp):
-                gathered(sqpk, k, ss_sem, sr_sem)
-                gathered(xpk, k, xs_sem.at[1], xr_sem.at[1])
-            xall[...] = dot(unpacker[...], xpk[...].reshape(packed, depth)).astype(BF16)
-            sqd[block, dp] = exact(jnp.sum(sqpk[...], axis=0), packer[...])
+                arrived(sqpk, ss_sem, sr_sem, source(k))
+            sqd[dp] = jnp.sum(sqpk[...], axis=0)
         for k in range(1, ndp):
             cp = remote(
-                sqd.at[block, dp], sqd.at[block, dp], qs_sem.at[block, k], qr_sem.at[block, k],
+                sqd.at[dp], sqd.at[dp], qs_sem.at[block, k], qr_sem.at[block, k],
                 "dp", lax.rem(dp + k, ndp),
             )
             cp.start()
             sends.append(cp)
 
-        def copy_a(c):
-            return remote(
-                send_a.at[block, c], recv_a.at[block, c], as_sem.at[block, c], ar_sem.at[block, c],
-                "dp", partner,
-            )
-
-        def copy_b(c, k):
-            xd = lax.rem(xpos + k, nx)
-            return remote(
-                send_b.at[block, c, k], recv_b.at[block, c, k],
-                bs_sem.at[block, c, k], br_sem.at[block, c, k],
-                "dp", CORES * xd + core,
-            )
-
-        def stage_b(c):
-            copy_a(c).wait_recv()
+        def late_b(n, carry):
+            stage_b(n)
+            return carry
+
+        lax.fori_loop(count - lag, count, late_b, 0)
+
+        def stage_c(n, carry):
+            j = lax.rem(n, pieces)
+            if first_block:
+                q = n // pieces
+                g = xpos * CORES * ratio + q
+                base = lax.rem(q, ratio) * size
+            else:
+                g = source(n // pieces)
+                base = g * size
+            total = part[g, j, my_half, :]
             for k in range(1, nx):
-                xd = lax.rem(xpos + k, nx)
-                send_b[block, c, k] = (
-                    part[c, CORES * xd + core] + recv_a[block, c, xd].astype(F32)
-                ).astype(BF16)
-                copy_b(c, k).start()
-
-        def first(c, carry):
-            pltpu.make_async_copy(wbuf.at[block, c], wbuf.at[block, c], wsem.at[block, c]).wait()
-            res = jnp.dot(xall[...], wbuf[block, c], preferred_element_type=F32)
-            part[c] = res.reshape(ndp, rows, width)
-            for xd in range(nx):
-                send_a[block, c, xd] = part[c, CORES * xd + 1 - core].astype(BF16)
-            copy_a(c).start()
-
-            @pl.when(c > 0)
-            def _():
-                stage_b(c - 1)
-
+                peer = lax.rem(xpos + k, nx)
+                copy_b(g, j, peer, peer).wait_recv()
+                total = total + recv_b[peer, g, j].astype(F32)
+            at = pl.ds(pl.multiple_of(base + core * half, half), half)
+            if first_block:
+                @pl.when(q // ratio == core)
+                def _():
+                    tot[j, at, :] = total
+
+                @pl.when(q // ratio != core)
+                def _():
+                    part[g, j, my_half, :] = total
+                    remote(
+                        part.at[g, j, my_half, :], tot.at[j, at, :],
+                        ds_sem.at[block, g * pieces + j], dr_sem.at[block, g * pieces + j],
+                        "dp", partner,
+                    ).start()
+            else:
+                tot[j, at, :] = total
+                copy_d(g, j).start()
             return carry
 
-        lax.fori_loop(0, chunks, first, 0)
-        stage_b(chunks - 1)
+        lax.fori_loop(0, CORES * ratio * pieces if first_block else count, stage_c, 0)
         for k in range(1, ndp):
             src = lax.rem(dp + ndp - k, ndp)
             remote(
-                sqd.at[block, src], sqd.at[block, src], qs_sem.at[block, k], qr_sem.at[block, k],
-                "dp", src,
+                sqd.at[src], sqd.at[src], qs_sem.at[block, k], qr_sem.at[block, k], "dp", src
             ).wait_recv()
-        total = exact(own_lanes, jnp.sum(sqd[block], axis=0), NT)[:, 0:1]
-        inv = lax.rsqrt(total / features + norm_eps)
-
-        def last(c, carry):
-            own = part[c, CORES * xpos + core] + recv_a[block, c, xpos].astype(F32)
-            for k in range(1, nx):
-                copy_b(c, k).wait_recv()
-                own = own + recv_b[block, c, k].astype(F32)
-            totals[:, pl.ds(pl.multiple_of(c * width, width), width)] = own * inv
-            copy_a(c).wait_send()
-            for k in range(1, nx):
-                copy_b(c, k).wait_send()
-            return carry
-
-        lax.fori_loop(0, chunks, last, 0)
-        if block == 0:
+        tall_index = rows if first_block else packed
+        wide_index = every if first_block else packed
+        begin = dp * rows if first_block else 0
+        lanes = jnp.where(
+            grid_of((tall_index, wide_index), 1) == grid_of((tall_index, wide_index), 0) + begin, 1.0, 0.0
+        )
+        inv = lax.rsqrt(exact(lanes, jnp.sum(sqd[...], axis=0), NT)[:, 0:1] / features + norm_eps)
+        if first_block:
+            to_own = own_spot
+        else:
+            to_own = dot(own_spot, unpacker[own_groups, :]).astype(BF16)
+        if first_block:
             loads[5].wait()
             loads[6].wait()
+
+        def expected(n, carry):
+            g = dp * ratio + n // pieces if first_block else source(n // pieces)
+            expect_d(g, lax.rem(n, pieces))
+            return carry
+
+        lax.fori_loop(0, ratio * pieces if first_block else count, expected, 0)
+
+        def projected(i):
+            cols = slice(i % each * span, (i % each + 1) * span)
+            return split_right(to_own, tot[i // each, :, cols] * inv)
+
         gated, update = mix(
-            steps, block,
-            [split_right(own_spot, totals[:, i * span : (i + 1) * span]) for i in range(6)],
+            steps, block, [projected(i) for i in range(6)],
             live, bases[block : block + 1, :], ogains[block : block + 1, :], state, final_ref, span,
             vals_s, seen_s, read_s, ask_s, on_s,
         )
@@ -426,29 +535,50 @@
             cp.start()
             sends.append(cp)
         update()
-        if block + 1 < BLOCKS:
-            current = dot(packer[part_rows, :], xg[...].reshape(every, depth))
+        if first_block:
+            current = dot(packer[mine_packed, :], xg[...].reshape(every, depth))
         else:
             back = dot(
                 unpacker[pl.ds(pl.multiple_of(tp * cap, cap), cap), :],
                 xpk[...].reshape(packed, depth),
             )
             current = back / gains[block : block + 1, :]
+
+        def settle(n, carry):
+            g, j = n // pieces, lax.rem(n, pieces)
+            copy_a(g, j).wait_send()
+            for k in range(1, nx):
+                peer = lax.rem(xpos + k, nx)
+                if first_block:
+                    @pl.when(chip_of(g) == peer)
+                    def _():
+                        copy_b(g, j, peer, xpos).wait_send()
+                else:
+                    copy_b(g, j, peer, xpos).wait_send()
+            if first_block:
+                @pl.when(g // ratio == partner)
+                def _():
+                    copy_d(g, j).wait_send()
+            else:
+                copy_d(g, j).wait_send()
+            return carry
+
+        lax.fori_loop(0, count, settle, 0)
         for k in range(1, ndp):
             src = lax.rem(dp + ndp - k, ndp)
             remote(
                 gg.at[block, src], gg.at[block, src], gs_sem.at[block, k], gr_sem.at[block, k], "dp", src
             ).wait_recv()
         rest = gg[block].reshape(every, span)
-        if block + 1 < BLOCKS:
+        if first_block:
             rest = dot(packer[...], rest).astype(BF16)
             sbuf, rbuf = psend, precv
         else:
             sbuf, rbuf = osend, orecv
-        size = sbuf.shape[1]
+        step_rows = sbuf.shape[1]
         partial = jnp.dot(rest, wobuf[block], preferred_element_type=F32)
         for g in range(ntp):
-            sbuf[g] = partial[g * size : (g + 1) * size].astype(BF16)
+            sbuf[g] = partial[g * step_rows : (g + 1) * step_rows].astype(BF16)
         back_sends = []
         for k in range(1, ntp):
             peer = lax.rem(tp + k, ntp)
@@ -459,7 +589,9 @@
             sends.append(cp)
             back_sends.append(cp)
         for g in range(ntp):
-            current = current + jnp.where(tp == g, partial[g * size : (g + 1) * size], 0.0)
+            current = current + jnp.where(
+                tp == g, partial[g * step_rows : (g + 1) * step_rows], 0.0
+            )
         for k in range(1, ntp):
             back_sends[k - 1].wait_recv()
             current = current + rbuf[k].astype(F32)
@@ -485,13 +617,15 @@
     rows = ntp // ndp * cap
     features = depth * ndp
     span = w_key.shape[2]
-    width = min(256, span)
-    chunks = 6 * span // width
+    pieces = 3
+    lag = 3
+    wide = 6 * span // pieces
     nx = ndp // CORES
     heads = span // HEAD
     tall = steps * heads
     every = ntp * cap
     packed = ntp * share
+    count = ntp * pieces
     dma = pltpu.SemaphoreType.DMA
     vmem = pl.BlockSpec(memory_space=pltpu.VMEM)
     hbm = pl.BlockSpec(memory_space=pl.ANY)
@@ -501,7 +635,7 @@
         return pltpu.VMEM(shape, dtype)
 
     return pl.pallas_call(
-        functools.partial(whole_kernel, ntp, ndp, steps, features, width, cap, share),
+        functools.partial(whole_kernel, ntp, ndp, steps, features, cap, share, lag),
         out_shape=(
             jax.ShapeDtypeStruct((seqs, steps, depth), F32),
             jax.ShapeDtypeStruct(states.shape, F32),
@@ -512,22 +646,23 @@
             buf(seqs, steps, depth, dtype=BF16),
             pltpu.SMEM(lengths.shape, jnp.int32),
             buf(B, depth), buf(B, span), buf(B, span),
-            buf(B, chunks, depth, width, dtype=BF16),
+            buf(B, 6, depth, span, dtype=BF16),
             buf(B, span, depth, dtype=BF16),
             buf(*states.shape),
             buf(ntp, cap, depth, dtype=BF16),
             buf(ntp, share, depth, dtype=BF16),
+            buf(cap, depth, dtype=BF16),
             buf(ntp, 8, packed),
-            buf(B, ndp, 8, every),
-            buf(packed, LANES),
-            buf(packed, every), buf(every, packed, dtype=BF16),
-            buf(every, depth, dtype=BF16),
-            buf(chunks, ndp, rows, width),
-            buf(B, chunks, nx, rows, width, dtype=BF16),
-            buf(B, chunks, nx, rows, width, dtype=BF16),
-            buf(B, chunks, nx, rows, width, dtype=BF16),
-            buf(B, chunks, nx, rows, width, dtype=BF16),
-            buf(rows, 6 * span),
+            buf(ndp, 8, every), buf(ndp, 8, packed),
+            buf(every, LANES), buf(packed, LANES),
+            buf(packed, every, dtype=BF16), buf(every, packed, dtype=BF16),
+            buf(ntp, pieces, cap, wide), buf(ntp, pieces, share, wide),
+            buf(ntp, pieces, cap // CORES, wide), buf(ntp, pieces, share // CORES, wide),
+            buf(ntp, pieces, cap // CORES, wide, dtype=BF16),
+            buf(ntp, pieces, share // CORES, wide, dtype=BF16),
+            buf(nx, ntp, pieces, cap // CORES, wide, dtype=BF16),
+            buf(nx, ntp, pieces, share // CORES, wide, dtype=BF16),
+            buf(pieces, rows, wide), buf(pieces, packed, wide),
             buf(B, ndp, rows, span, dtype=BF16),
             buf(ntp, cap, depth, dtype=BF16),
             buf(ntp, cap, depth, dtype=BF16),
@@ -535,10 +670,11 @@
             buf(ntp, share, depth, dtype=BF16),
             buf(held * tall, LANES), buf(held * tall, LANES), buf(held * tall, LANES),
             buf(held, 2 * tall, span, dtype=BF16), buf(held, 2 * tall, LANES),
-            dma((7,)), dma((B, chunks)),
+            dma((7,)), dma((B, 6)),
             dma((2, ntp)), dma((2, ntp)), dma((ntp,)), dma((ntp,)),
-            dma((B, chunks)), dma((B, chunks)),
-            dma((B, chunks, nx)), dma((B, chunks, nx)),
+            dma((B, count)), dma((B, count)),
+            dma((B, nx, count)), dma((B, nx, count)),
+            dma((B, count)), dma((B, count)),
             dma((B, ndp)), dma((B, ndp)),
             dma((B, ndp)), dma((B, ndp)), dma((B, ntp)), dma((B, ntp)),
         ],

time: 94.5 us -> 93 us (0.984)
  Pallas kernels: 88.9 us -> 87.3 us
    pallas_call x1, Pallas kernels: 88.9 us -> 87.3 us  [body(): pl.pallas_call(functools.partial(whole_kernel, ntp, ndp, steps, features,...]
where the time goes in v3:
time: 93 us; the launch traced here: 92.8 us
  Pallas kernels  87.3 us (94%)
  local copies, waits for them, and re-layouts  4.81 us (5%)
    pallas_call x1, Pallas kernels, body(): pl.pallas_call(functools.partial(whole_kernel, ntp, ndp, steps, features,...  87.3 us
    unnamed x2, local copies, waits for them, and re-layouts  4.81 us

profile of v3, /device:TPU:15, one launch (start us, length us, event | category | flops | bytes accessed | tf_op | source)
XLA Modules:
  0.0 92.8 jit_solution(13773188315968395695)
XLA Ops:
  0.6 87.3 %whole.1 = (f32[8,8,1024]{2,1,0:T(8,128)}, f32[2,8,64,512]{3,2,1,0:T(8,128)}) custom-call(bf16[8,8,1024]{2,1,0:T(8,128)(2,1)} %tokens.1, s32[32]{0:T(128)} %lengths.1, f32[2,1024]{1,0:T(2,128)} %norm_gain.1, bf16[2,1024,512]{2,1,0:T(8,128)(2,1)} %w0.1, bf16[2,1024,512]{2,1,0:T(8,128)(2,1)} %w1.1, bf16[2,1024,512]{2,1,0:T(8,128)(2,1)} %w2.1, ...), custom_call_target="tpu_custom_call" | custom-call | tf_op jit(solution)/shard_map/whole/pallas_call | solution.py:637
  88.0 1.7 %copy.17 = f32[8,8,1024]{2,1,0:T(8,128)} copy(f32[8,8,1024]{2,1,0:T(8,128)} %get-tuple-element.4) | data formatting | bytes 524288
  89.6 3.1 %copy.18 = f32[2,8,64,512]{3,2,1,0:T(8,128)} copy(f32[2,8,64,512]{3,2,1,0:T(8,128)} %get-tuple-element.5) | data formatting | bytes 4194304

commit v4 on v3

--- a/solution.py
+++ b/solution.py
@@ -85,7 +85,7 @@
 
 
 def mix(
-    steps, block, projected, live, base, gain, state, final, span,
+    steps, block, begin, projected, live, base, gain, state, final, span,
     vals_s, seen_s, read_s, ask_s, on_s,
 ):
     recept, keys, values, decay_pre, rate_pre, gate_pre = projected
@@ -140,7 +140,7 @@
         ends.append(grow[(b + 1) * steps - 1 : (b + 1) * steps])
     for b in range(held):
         cut = slice(b * steps, (b + 1) * steps)
-        against = jnp.concatenate([state[block, b], r_out[cut], k_out[cut], pad], axis=0)
+        against = jnp.concatenate([state[block, begin + b], r_out[cut], k_out[cut], pad], axis=0)
         on_s[b] = dot(ask_s[b], against, NT)
 
     for b in range(held):
@@ -185,7 +185,7 @@
             right = jnp.concatenate(
                 [spread(k_out[cut] * ends[b]), spread(r_out[cut] * ends[b])], axis=0
             )
-            final[block, b] = state[block, b] * ends[b] + dot(left, right, TN)[0:HEAD]
+            final[block, begin + b] = state[block, begin + b] * ends[b] + dot(left, right, TN)[0:HEAD]
 
     return gated, update
 
@@ -196,10 +196,10 @@
 
 
 def whole_kernel(
-    ntp, ndp, steps, features, cap, share, lag,
+    ntp, ndp, steps, features, cap, share, lag, halves,
     tokens, lengths, norm_gain, w0, w1, w2, w3, w4, w5, w_out, base_in, gain_in, states,
     out_ref, final_ref,
-    xtok, lens, gains, bases, ogains, wbuf, wobuf, state,
+    lens, gains, bases, ogains, wbuf, wobuf, state,
     xg, xpk, xs, sqpk, sqd0, sqd1, acc0, acc1, packer, unpacker,
     part0, part1, recv_a0, recv_a1, send_b0, send_b1, recv_b0, recv_b1, tot0, tot1,
     gg, osend, orecv, psend, precv,
@@ -213,9 +213,8 @@
     pieces, rows, wide = tot0.shape
     each = wide // span
     held = state.shape[1]
-    seqs = xtok.shape[0]
     ratio = ntp // ndp
-    here = seqs * steps
+    seqs = cap // steps
     every = ntp * cap
     packed = ntp * share
     nx = ndp // CORES
@@ -230,7 +229,7 @@
         pltpu.make_async_copy(src, dst, load_sem.at[i])
         for i, (src, dst) in enumerate(
             (
-                (tokens, xtok), (lengths, lens), (norm_gain, gains), (base_in, bases),
+                (tokens, xg.at[tp]), (lengths, lens), (norm_gain, gains), (base_in, bases),
                 (gain_in, ogains), (states, state), (w_out, wobuf),
             )
         )
@@ -254,27 +253,6 @@
     )
     for cp in loads[:2]:
         cp.wait()
-
-    def spot(first, number):
-        index = grid_of((number * steps, 1), 0)
-        at, starts, counts = jnp.int32(0), [], []
-        for b in range(number):
-            if b % seqs == 0:
-                at = jnp.int32(b // seqs * cap)
-            starts.append(at)
-            counts.append(lens[first + b])
-            at = at + counts[-1]
-        step = index % steps
-        place = by_index(starts, index // steps) + step
-        alive = step < by_index(counts, index // steps)
-        shape = (number * steps, number // seqs * cap)
-        one = jnp.where((place == grid_of(shape, 1)) & alive, 1.0, 0.0)
-        return one, jnp.where(alive, 1.0, 0.0)
-
-    mine, mine_live = spot(tp * seqs, seqs)
-    mine = mine.astype(BF16)
-    flat_tokens = xtok[...].reshape(here, depth)
-    xg[tp] = dot(mine, flat_tokens, TN).astype(BF16)
     sends = []
 
     order = near_first(ntp)
@@ -300,27 +278,30 @@
 
     spread_out(xg, xs_sem.at[0], xr_sem.at[0])
 
-    own_spot, live = spot(dp * held, held)
-    own_spot = own_spot.astype(BF16)
+    def alive(first, number, rows_here):
+        index = grid_of((rows_here, 1), 0)
+        return index % steps < by_index([lens[first + b] for b in range(number)], index // steps)
+
+    live = jnp.where(alive(dp * held, held, rows), 1.0, 0.0)
     starts, counts, at = [], [], jnp.int32(0)
-    for g in range(ntp):
+    for b in range(ntp * seqs):
         starts.append(at)
-        number = jnp.int32(0)
-        for b in range(seqs):
-            number = number + lens[g * seqs + b]
-        counts.append(number)
-        at = at + number
+        counts.append(lens[b])
+        at = at + counts[-1]
 
     def ranks(index):
+        step = index % steps
         return jnp.where(
-            index % cap < by_index(counts, index // cap),
-            by_index(starts, index // cap) + index % cap,
-            -1,
+            step < by_index(counts, index // steps), by_index(starts, index // steps) + step, -1
         )
 
-    packer[...] = jnp.where(
-        grid_of((packed, every), 0) == ranks(grid_of((1, every), 1)), 1.0, 0.0
-    ).astype(BF16)
+    for h in range(halves):
+        column = grid_of((1, every // halves), 1)
+        natural = column // (cap // halves) * cap + h * (cap // halves) + column % (cap // halves)
+        packer[h] = jnp.where(
+            grid_of((packed, every // halves), 0) == ranks(natural), 1.0, 0.0
+        ).astype(BF16)
+    still = alive(tp * seqs, seqs, cap)
     unpacker[...] = jnp.where(
         ranks(grid_of((every, 1), 0)) == grid_of((every, packed), 1), 1.0, 0.0
     ).astype(BF16)
@@ -328,6 +309,7 @@
     ones = jnp.ones((8, LANES), F32)
     for cp in loads[2:5]:
         cp.wait()
+    thin = cap // halves
     mine_packed = pl.ds(pl.multiple_of(tp * share, share), share)
     own_groups = pl.ds(pl.multiple_of(dp * rows, rows), rows)
     current = None
@@ -503,10 +485,6 @@
         )
         inv = lax.rsqrt(exact(lanes, jnp.sum(sqd[...], axis=0), NT)[:, 0:1] / features + norm_eps)
         if first_block:
-            to_own = own_spot
-        else:
-            to_own = dot(own_spot, unpacker[own_groups, :]).astype(BF16)
-        if first_block:
             loads[5].wait()
             loads[6].wait()
 
@@ -517,26 +495,41 @@
 
         lax.fori_loop(0, ratio * pieces if first_block else count, expected, 0)
 
-        def projected(i):
+        def projected(i, band):
             cols = slice(i % each * span, (i % each + 1) * span)
-            return split_right(to_own, tot[i // each, :, cols] * inv)
-
-        gated, update = mix(
-            steps, block, [projected(i) for i in range(6)],
-            live, bases[block : block + 1, :], ogains[block : block + 1, :], state, final_ref, span,
-            vals_s, seen_s, read_s, ask_s, on_s,
-        )
-        gg[block, dp] = dot(own_spot, gated, TN).astype(BF16)
-        for k in range(1, ndp):
-            cp = remote(
-                gg.at[block, dp], gg.at[block, dp], gs_sem.at[block, k], gr_sem.at[block, k],
-                "dp", lax.rem(dp + k, ndp),
-            )
-            cp.start()
-            sends.append(cp)
-        update()
+            if first_block:
+                return tot[i // each, band, cols] * inv[band]
+            take = pl.ds(pl.multiple_of(dp * rows + band.start, band.stop - band.start), band.stop - band.start)
+            return split_right(unpacker[take, :], tot[i // each, :, cols] * inv)
+
+        def share_out(h, k, peer, at):
+            return remote(
+                gg.at[block, h, at], gg.at[block, h, at], gs_sem.at[block, h, k], gr_sem.at[block, h, k],
+                "dp", peer,
+            )
+
+        updates = []
+        for h in range(halves):
+            band = slice(h * rows // halves, (h + 1) * rows // halves)
+            gated, update = mix(
+                steps, block, h * held // halves, [projected(i, band) for i in range(6)],
+                live[band], bases[block : block + 1, :], ogains[block : block + 1, :],
+                state, final_ref, span,
+                vals_s.at[h], seen_s.at[h], read_s.at[h], ask_s.at[h], on_s.at[h],
+            )
+            updates.append(update)
+            gg[block, h, dp] = gated
+            for k in range(1, ndp):
+                cp = share_out(h, k, lax.rem(dp + k, ndp), dp)
+                cp.start()
+                sends.append(cp)
+        for update in updates:
+            update()
         if first_block:
-            current = dot(packer[mine_packed, :], xg[...].reshape(every, depth))
+            current = 0.0
+            for h in range(halves):
+                rows_h = xg[:, h * thin : (h + 1) * thin, :].reshape(every // halves, depth)
+                current = current + dot(packer[h, mine_packed, :], rows_h)
         else:
             back = dot(
                 unpacker[pl.ds(pl.multiple_of(tp * cap, cap), cap), :],
@@ -564,41 +557,55 @@
             return carry
 
         lax.fori_loop(0, count, settle, 0)
-        for k in range(1, ndp):
-            src = lax.rem(dp + ndp - k, ndp)
-            remote(
-                gg.at[block, src], gg.at[block, src], gs_sem.at[block, k], gr_sem.at[block, k], "dp", src
-            ).wait_recv()
-        rest = gg[block].reshape(every, span)
+        def shared(h):
+            for k in range(1, ndp):
+                src = lax.rem(dp + ndp - k, ndp)
+                share_out(h, k, src, src).wait_recv()
+
+        def give(h, left, sbuf, rbuf):
+            partial = jnp.dot(left, wobuf[block], preferred_element_type=F32)
+            many = partial.shape[0] // ntp
+            for g in range(ntp):
+                sbuf[h, g] = partial[g * many : (g + 1) * many].astype(BF16)
+            started = []
+            for k in range(1, ntp):
+                peer = lax.rem(tp + k, ntp)
+                cp = remote(
+                    sbuf.at[h, peer], rbuf.at[h, k],
+                    os_sem.at[block, h, k], or_sem.at[block, h, k], "tp", peer,
+                )
+                cp.start()
+                started.append(cp)
+            sends.extend(started)
+            own = jnp.zeros((many, depth), F32)
+            for g in range(ntp):
+                own = own + jnp.where(tp == g, partial[g * many : (g + 1) * many], 0.0)
+            return own, started
+
         if first_block:
-            rest = dot(packer[...], rest).astype(BF16)
-            sbuf, rbuf = psend, precv
+            for h in range(halves):
+                shared(h)
+            left = 0.0
+            for h in range(halves):
+                left = left + dot(packer[h], gg[block, h].reshape(every // halves, span))
+            own, started = give(0, left.astype(BF16), psend, precv)
+            current = current + own
+            for k in range(1, ntp):
+                started[k - 1].wait_recv()
+                current = current + precv[0, k].astype(F32)
         else:
-            sbuf, rbuf = osend, orecv
-        step_rows = sbuf.shape[1]
-        partial = jnp.dot(rest, wobuf[block], preferred_element_type=F32)
-        for g in range(ntp):
-            sbuf[g] = partial[g * step_rows : (g + 1) * step_rows].astype(BF16)
-        back_sends = []
-        for k in range(1, ntp):
-            peer = lax.rem(tp + k, ntp)
-            cp = remote(
-                sbuf.at[peer], rbuf.at[k], os_sem.at[block, k], or_sem.at[block, k], "tp", peer
-            )
-            cp.start()
-            sends.append(cp)
-            back_sends.append(cp)
-        for g in range(ntp):
-            current = current + jnp.where(
-                tp == g, partial[g * step_rows : (g + 1) * step_rows], 0.0
-            )
-        for k in range(1, ntp):
-            back_sends[k - 1].wait_recv()
-            current = current + rbuf[k].astype(F32)
-    result = jnp.where(
-        mine_live > 0, exact(mine.astype(F32), current), flat_tokens.astype(F32)
-    )
-    out_ref[...] = result.reshape(out_ref.shape)
+            given = []
+            for h in range(halves):
+                shared(h)
+                given.append(give(h, gg[block, h].reshape(every // halves, span), osend, orecv))
+            for h in range(halves):
+                own, started = given[h]
+                cut = slice(h * thin, (h + 1) * thin)
+                total = current[cut] + own
+                for k in range(1, ntp):
+                    started[k - 1].wait_recv()
+                    total = total + orecv[h, k].astype(F32)
+                out_ref[cut, :] = jnp.where(still[cut], total, xg[tp, cut, :].astype(F32))
     for cp in sends:
         cp.wait_send()
 
@@ -617,8 +624,9 @@
     rows = ntp // ndp * cap
     features = depth * ndp
     span = w_key.shape[2]
-    pieces = 3
-    lag = 3
+    pieces = 2
+    lag = 1
+    halves = 2 if ntp == ndp and held % 2 == 0 else 1
     wide = 6 * span // pieces
     nx = ndp // CORES
     heads = span // HEAD
@@ -634,16 +642,15 @@
     def buf(*shape, dtype=F32):
         return pltpu.VMEM(shape, dtype)
 
-    return pl.pallas_call(
-        functools.partial(whole_kernel, ntp, ndp, steps, features, cap, share, lag),
+    stream, finals = pl.pallas_call(
+        functools.partial(whole_kernel, ntp, ndp, steps, features, cap, share, lag, halves),
         out_shape=(
-            jax.ShapeDtypeStruct((seqs, steps, depth), F32),
-            jax.ShapeDtypeStruct(states.shape, F32),
+            pltpu.VMEM((cap, depth), F32),
+            pltpu.VMEM(states.shape, F32),
         ),
         in_specs=[hbm] * 13,
         out_specs=(vmem, vmem),
         scratch_shapes=[
-            buf(seqs, steps, depth, dtype=BF16),
             pltpu.SMEM(lengths.shape, jnp.int32),
             buf(B, depth), buf(B, span), buf(B, span),
             buf(B, 6, depth, span, dtype=BF16),
@@ -655,7 +662,7 @@
             buf(ntp, 8, packed),
             buf(ndp, 8, every), buf(ndp, 8, packed),
             buf(every, LANES), buf(packed, LANES),
-            buf(packed, every, dtype=BF16), buf(every, packed, dtype=BF16),
+            buf(halves, packed, every // halves, dtype=BF16), buf(every, packed, dtype=BF16),
             buf(ntp, pieces, cap, wide), buf(ntp, pieces, share, wide),
             buf(ntp, pieces, cap // CORES, wide), buf(ntp, pieces, share // CORES, wide),
             buf(ntp, pieces, cap // CORES, wide, dtype=BF16),
@@ -663,30 +670,39 @@
             buf(nx, ntp, pieces, cap // CORES, wide, dtype=BF16),
             buf(nx, ntp, pieces, share // CORES, wide, dtype=BF16),
             buf(pieces, rows, wide), buf(pieces, packed, wide),
-            buf(B, ndp, rows, span, dtype=BF16),
-            buf(ntp, cap, depth, dtype=BF16),
-            buf(ntp, cap, depth, dtype=BF16),
-            buf(ntp, share, depth, dtype=BF16),
-            buf(ntp, share, depth, dtype=BF16),
-            buf(held * tall, LANES), buf(held * tall, LANES), buf(held * tall, LANES),
-            buf(held, 2 * tall, span, dtype=BF16), buf(held, 2 * tall, LANES),
+            buf(B, halves, ndp, rows // halves, span, dtype=BF16),
+            buf(halves, ntp, cap // halves, depth, dtype=BF16),
+            buf(halves, ntp, cap // halves, depth, dtype=BF16),
+            buf(1, ntp, share, depth, dtype=BF16),
+            buf(1, ntp, share, depth, dtype=BF16),
+            buf(halves, held * tall // halves, LANES),
+            buf(halves, held * tall // halves, LANES),
+            buf(halves, held * tall // halves, LANES),
+            buf(halves, held // halves, 2 * tall, span, dtype=BF16),
+            buf(halves, held // halves, 2 * tall, LANES),
             dma((7,)), dma((B, 6)),
             dma((2, ntp)), dma((2, ntp)), dma((ntp,)), dma((ntp,)),
             dma((B, count)), dma((B, count)),
             dma((B, nx, count)), dma((B, nx, count)),
             dma((B, count)), dma((B, count)),
             dma((B, ndp)), dma((B, ndp)),
-            dma((B, ndp)), dma((B, ndp)), dma((B, ntp)), dma((B, ntp)),
+            dma((B, halves, ndp)), dma((B, halves, ndp)), dma((B, halves, ntp)), dma((B, halves, ntp)),
         ],
         compiler_params=pltpu.CompilerParams(
-            collective_id=0, has_side_effects=True, vmem_limit_bytes=60 * 1024 * 1024
+            collective_id=0, has_side_effects=True, vmem_limit_bytes=56 * 1024 * 1024
         ),
         name="whole",
     )(
-        tokens, lengths, norm_gain,
-        w_recept, w_key, w_value, w_decay, w_rate, w_gate,
-        w_out, decay_base, out_gain, states,
+        *(
+            pltpu.with_memory_space_constraint(a, pltpu.HBM)
+            for a in (
+                tokens.reshape(cap, depth), lengths, norm_gain,
+                w_recept, w_key, w_value, w_decay, w_rate, w_gate,
+                w_out, decay_base, out_gain, states,
+            )
+        )
     )
+    return stream.reshape(tokens.shape), finals
 
 
 def solution(mesh):

time: 93 us -> 86 us (0.925)
  Pallas kernels: 87.3 us -> 82.4 us
  local copies, waits for them, and re-layouts: 4.81 us -> 2.02 us
    pallas_call x1, Pallas kernels: 87.3 us -> 82.4 us  [body(): pl.pallas_call(functools.partial(whole_kernel, ntp, ndp, steps, features,...]
    unnamed x2, local copies, waits for them, and re-layouts: 4.81 us -> 2.02 us
where the time goes in v4:
time: 86 us; the launch traced here: 85 us
  Pallas kernels  82.4 us (96%)
  local copies, waits for them, and re-layouts  2.02 us (2%)
    pallas_call x1, Pallas kernels, body(): pl.pallas_call(functools.partial(whole_kernel, ntp, ndp, steps, features,...  82.4 us
    unnamed x2, local copies, waits for them, and re-layouts  2.02 us

profile of v4, /device:TPU:15, one launch (start us, length us, event | category | flops | bytes accessed | tf_op | source)
XLA Modules:
  0.0 85.0 jit_solution(8573828623937460064)
XLA Ops:
  0.6 82.4 %whole.1 = (f32[64,1024]{1,0:T(8,128)S(1)}, f32[2,8,64,512]{3,2,1,0:T(8,128)S(1)}) custom-call(bf16[64,1024]{1,0:T(8,128)(2,1)} %bitcast.3, s32[32]{0:T(128)} %lengths.1, f32[2,1024]{1,0:T(2,128)} %norm_gain.1, bf16[2,1024,512]{2,1,0:T(8,128)(2,1)} %w0.1, bf16[2,1024,512]{2,1,0:T(8,128)(2,1)} %w1.1, bf16[2,1024,512]{2,1,0:T(8,128)(2,1)} %w2.1, ...), custom_call_target="tpu_custom_call" | custom-call | tf_op jit(solution)/shard_map/whole/pallas_call | solution.py:645
  83.0 0.7 copy.17
  83.7 1.3 %copy.18 = f32[2,8,64,512]{3,2,1,0:T(8,128)} copy(f32[2,8,64,512]{3,2,1,0:T(8,128)S(1)} %get-tuple-element.7) | data formatting | bytes 4194304

commit v5 on v4

--- a/solution.py
+++ b/solution.py
@@ -196,7 +196,7 @@
 
 
 def whole_kernel(
-    ntp, ndp, steps, features, cap, share, lag, halves,
+    ntp, ndp, steps, features, cap, share, live_rows, lag, halves,
     tokens, lengths, norm_gain, w0, w1, w2, w3, w4, w5, w_out, base_in, gain_in, states,
     out_ref, final_ref,
     lens, gains, bases, ogains, wbuf, wobuf, state,
@@ -306,6 +306,10 @@
         ranks(grid_of((every, 1), 0)) == grid_of((every, packed), 1), 1.0, 0.0
     ).astype(BF16)
     acc1[...] = jnp.zeros_like(acc1)
+    clear = -(-live_rows // (share // CORES)) * (share // CORES)
+    if clear < packed:
+        for j in range(pieces):
+            tot1[j, clear:, :] = jnp.zeros((packed - clear, wide), F32)
     ones = jnp.ones((8, LANES), F32)
     for cp in loads[2:5]:
         cp.wait()
@@ -364,7 +368,19 @@
                 "dp", partner,
             ).wait_recv()
 
+        def used(g, c):
+            return first_block or g * size + c * half < live_rows
+
+        def guarded(test, action):
+            if test is True:
+                action()
+            else:
+                pl.when(test)(action)
+
         def stage_b(n):
+            guarded(used(source(n // pieces), core), lambda: combine(n))
+
+        def combine(n):
             g, j = source(n // pieces), lax.rem(n, pieces)
             copy_a(g, j).wait_recv()
             total = part[g, j, my_half, :] + recv_a[g, j]
@@ -409,7 +425,7 @@
                 part[g, j, :, c * span : (c + 1) * span] = jnp.dot(
                     left, wbuf[block, j * each + c], preferred_element_type=F32
                 )
-            copy_a(g, j).start()
+            guarded(used(g, 1 - core), lambda: copy_a(g, j).start())
 
             @pl.when(n >= lag)
             def _():
@@ -418,6 +434,11 @@
             return carry
 
         lax.fori_loop(0, count, stage_a, 0)
+        def late_b(n, carry):
+            stage_b(n)
+            return carry
+
+        lax.fori_loop(count - lag, count, late_b, 0)
         if first_block:
             sqd[dp] = exact(ones, acc0[...], NT)
         else:
@@ -432,13 +453,12 @@
             cp.start()
             sends.append(cp)
 
-        def late_b(n, carry):
-            stage_b(n)
+        def stage_c(n, carry):
+            g = 0 if first_block else source(n // pieces)
+            guarded(used(g, core), lambda: finish(n))
             return carry
 
-        lax.fori_loop(count - lag, count, late_b, 0)
-
-        def stage_c(n, carry):
+        def finish(n):
             j = lax.rem(n, pieces)
             if first_block:
                 q = n // pieces
@@ -469,7 +489,6 @@
             else:
                 tot[j, at, :] = total
                 copy_d(g, j).start()
-            return carry
 
         lax.fori_loop(0, CORES * ratio * pieces if first_block else count, stage_c, 0)
         for k in range(1, ndp):
@@ -490,7 +509,7 @@
 
         def expected(n, carry):
             g = dp * ratio + n // pieces if first_block else source(n // pieces)
-            expect_d(g, lax.rem(n, pieces))
+            guarded(used(g, 1 - core), lambda: expect_d(g, lax.rem(n, pieces)))
             return carry
 
         lax.fori_loop(0, ratio * pieces if first_block else count, expected, 0)
@@ -539,21 +558,25 @@
 
         def settle(n, carry):
             g, j = n // pieces, lax.rem(n, pieces)
-            copy_a(g, j).wait_send()
-            for k in range(1, nx):
-                peer = lax.rem(xpos + k, nx)
+            guarded(used(g, 1 - core), lambda: copy_a(g, j).wait_send())
+
+            def sent():
+                for k in range(1, nx):
+                    peer = lax.rem(xpos + k, nx)
+                    if first_block:
+                        @pl.when(chip_of(g) == peer)
+                        def _():
+                            copy_b(g, j, peer, xpos).wait_send()
+                    else:
+                        copy_b(g, j, peer, xpos).wait_send()
                 if first_block:
-                    @pl.when(chip_of(g) == peer)
+                    @pl.when(g // ratio == partner)
                     def _():
-                        copy_b(g, j, peer, xpos).wait_send()
+                        copy_d(g, j).wait_send()
                 else:
-                    copy_b(g, j, peer, xpos).wait_send()
-            if first_block:
-                @pl.when(g // ratio == partner)
-                def _():
                     copy_d(g, j).wait_send()
-            else:
-                copy_d(g, j).wait_send()
+
+            guarded(used(g, core), sent)
             return carry
 
         lax.fori_loop(0, count, settle, 0)
@@ -643,7 +666,7 @@
         return pltpu.VMEM(shape, dtype)
 
     stream, finals = pl.pallas_call(
-        functools.partial(whole_kernel, ntp, ndp, steps, features, cap, share, lag, halves),
+        functools.partial(whole_kernel, ntp, ndp, steps, features, cap, share, live_rows, lag, halves),
         out_shape=(
             pltpu.VMEM((cap, depth), F32),
             pltpu.VMEM(states.shape, F32),

time: 86 us -> 84.8 us (0.986)
  Pallas kernels: 82.4 us -> 80.7 us
    pallas_call x1, Pallas kernels: 82.4 us -> 80.7 us  [body(): pl.pallas_call(functools.partial(whole_kernel, ntp, ndp, steps, features,...]
where the time goes in v5:
time: 84.8 us; the launch traced here: 83.4 us
  Pallas kernels  80.7 us (95%)
  local copies, waits for them, and re-layouts  2.02 us (2%)
    pallas_call x1, Pallas kernels, body(): pl.pallas_call(functools.partial(whole_kernel, ntp, ndp, steps, features,...  80.7 us
    unnamed x2, local copies, waits for them, and re-layouts  2.02 us

profile of v5, /device:TPU:15, one launch (start us, length us, event | category | flops | bytes accessed | tf_op | source)
XLA Modules:
  0.0 83.4 jit_solution(16484209496034544445)
XLA Ops:
  0.6 80.7 %whole.1 = (f32[64,1024]{1,0:T(8,128)S(1)}, f32[2,8,64,512]{3,2,1,0:T(8,128)S(1)}) custom-call(bf16[64,1024]{1,0:T(8,128)(2,1)} %bitcast.3, s32[32]{0:T(128)} %lengths.1, f32[2,1024]{1,0:T(2,128)} %norm_gain.1, bf16[2,1024,512]{2,1,0:T(8,128)(2,1)} %w0.1, bf16[2,1024,512]{2,1,0:T(8,128)(2,1)} %w1.1, bf16[2,1024,512]{2,1,0:T(8,128)(2,1)} %w2.1, ...), custom_call_target="tpu_custom_call" | custom-call | tf_op jit(solution)/shard_map/whole/pallas_call | solution.py:668
  81.4 0.7 copy.17
  82.1 1.3 %copy.18 = f32[2,8,64,512]{3,2,1,0:T(8,128)} copy(f32[2,8,64,512]{3,2,1,0:T(8,128)S(1)} %get-tuple-element.7) | data formatting | bytes 4194304
